TPU v7x, 1024 devices: a whole 4x4x32 slice. The times are simulated.
1024 devices in a mesh: rep: 4 (over z_hi), fs: 32 (over z_lo, y), tp: 8 (over x, core).
Axes of the slice: x: 4, y: 4, z: 32 (z_hi: 4, z_lo: 8; z = z_hi * 8 + z_lo), core: 2. Of those that a mesh axis runs over, the one named last changes fastest.
Arguments:
- stream: bfloat16 [32768, 2048], P(('rep', 'fs')), may hold values from -6 to 6
- gain_mix: float32 [2048], replicated, may hold values from 0.1 to 1.9
- w_query: float32 [2048, 2048], P('fs', 'tp'), may hold values from -0.125 to 0.125
- scale_query: float32 [2048], P('tp'), may hold values from 0.5 to 2
- w_key: float32 [2048, 2048], P('fs', 'tp'), may hold values from -0.125 to 0.125
- scale_key: float32 [2048], P('tp'), may hold values from 0.5 to 2
- w_value: float32 [2048, 2048], P('fs', 'tp'), may hold values from -0.125 to 0.125
- scale_value: float32 [2048], P('tp'), may hold values from 0.5 to 2
- gain_ffn: float32 [2048], replicated, may hold values from 0.1 to 1.9
- w_gate: float32 [2048, 2816], P('fs', 'tp'), may hold values from -0.125 to 0.125
- scale_gate: float32 [2816], P('tp'), may hold values from 0.5 to 2
- w_up: float32 [2048, 2816], P('fs', 'tp'), may hold values from -0.125 to 0.125
- scale_up: float32 [2816], P('tp'), may hold values from 0.5 to 2
- w_down: float32 [2048, 2816], P('fs', 'tp'), may hold values from -0.109375 to 0.109375
- scale_down: float32 [2048], P('fs'), may hold values from 0.5 to 2
Outputs:
- layer_out: bfloat16 [32768, 2048], P(('rep', 'fs', 'tp'))
All inputs are finite; a program needn't handle non-finite values.
Results may differ from a plain program's by a relative error of at most 0.015.
Values may be sent and summed in bfloat16 or wider, within the bound.
No kernel may reach another device: no remote copies, remote signals or barrier semaphores. Data moves between devices by JAX's collectives and lax.ppermute only.
A program may use at most 32 MiB of HBM per device.

v0:
```python
import jax
import jax.numpy as jnp
import numpy as np
from jax import lax
from jax.experimental import pallas as pl
from jax.experimental.pallas import tpu as pltpu
from jax.sharding import Mesh
from jax.sharding import PartitionSpec as P


EPS = 1e-06
THETA = 10000.0
HIGH = lax.Precision.HIGHEST
LEN = 128
Z = ("zh", "zl")
TP = ("x", "c")
F32 = jnp.float32
BF16 = jnp.bfloat16
VMEM = pl.BlockSpec(memory_space=pltpu.VMEM)
SMEM = pl.BlockSpec(memory_space=pltpu.SMEM)
MIB = 1 << 20


def shift(array, axis, offset):
    n = lax.axis_size(axis)
    return lax.ppermute(array, axis, [((i + offset) % n, i) for i in range(n)])


def call(kernel, out_shape, *args, scratch=(), specs=None, limit=6):
    return pl.pallas_call(
        kernel,
        out_shape=out_shape,
        in_specs=specs or [VMEM] * len(args),
        out_specs=jax.tree.map(lambda _: VMEM, out_shape),
        scratch_shapes=list(scratch),
        compiler_params=pltpu.CompilerParams(vmem_limit_bytes=limit * MIB),
    )(*args)


def pack_kernel(*refs):
    sources, qkv, ffn, held, sems = refs[:7], refs[7], refs[8], refs[9:16], refs[16]
    copies = [pltpu.make_async_copy(sources[i], held[i], sems.at[i]) for i in range(7)]
    for copy in copies:
        copy.start()
    copies[6].wait()
    diagonal = lax.broadcasted_iota(jnp.int32, (64, 64), 0) == lax.broadcasted_iota(jnp.int32, (64, 64), 1)
    scale = jnp.sum(jnp.where(diagonal, held[6][...], 0.0), axis=1, keepdims=True)
    high = scale.astype(BF16).astype(F32)
    middle = (scale - high).astype(BF16).astype(F32)
    low = scale - high - middle
    lane = lax.broadcasted_iota(jnp.int32, (64, 384), 1)
    extra = jnp.where(lane == 352, high, jnp.where(lane == 353, middle, jnp.where(lane == 354, low, 0.0)))
    extra = extra.astype(BF16)
    ffn[0:64, :] = jnp.zeros((64, 768), BF16)
    ffn[64:96, 0:384] = extra[0:32]
    ffn[64:96, 384:768] = extra[32:64]
    for copy in copies[:6]:
        copy.wait()
    wq, wk, wv, wg, wu, wd = held[:6]
    for copy in range(4):
        qkv[copy, :, 0:256] = wq[...].astype(BF16)
        qkv[copy, :, 256:512] = wk[...].astype(BF16)
        qkv[copy, :, 512:768] = wv[...].astype(BF16)
    ffn[0:64, 0:352] = wg[...].astype(BF16)
    ffn[0:64, 384:736] = wu[...].astype(BF16)
    down = wd[...].astype(BF16)
    ffn[64:96, 0:352] = down[0:32]
    ffn[64:96, 384:736] = down[32:64]


def first_kernel(qkv, fp1, fm1, plus, minus):
    plus[0:256, :] = qkv[...]
    plus[256:352, :] = fp1[...]
    minus[0:256, :] = qkv[...]
    minus[256:304, :] = fm1[48:96, :]
    minus[304:352, :] = fm1[0:48, :]


def batch_a_kernel(own, fp1, fm1, p1, m1, out):
    out[0:96, :] = own[...]
    out[96:192, :] = fp1[...]
    out[192:288, :] = fm1[...]
    out[288:384, :] = p1[256:352, :]
    out[384:432, :] = m1[304:352, :]
    out[432:480, :] = m1[256:304, :]


def batch_b_kernel(p2, m2, p3, m3, ap, am, plus, minus):
    for out in (plus, minus):
        out[0:96, :] = p2[256:352, :]
        out[96:144, :] = m2[304:352, :]
        out[144:192, :] = m2[256:304, :]
        out[192:240, :] = p3[256:304, :]
        out[240:288, :] = m3[256:304, :]
    plus[288:528, :] = ap[0:240, :]
    minus[288:528, :] = am[240:480, :]


def retention_kernel(decays, normed, own, p1, m1, p2, m2, p3, m3, p4, m4, sq, sk, sv, cosine, sine, out):
    zl = lax.axis_index("zl")
    decay = decays[lax.axis_index(TP)]
    acc = jnp.zeros((256, 768), F32)
    far = jnp.concatenate([p4[...], m4[...]], axis=0)
    blocks = {0: own, 1: p1, -1: m1, 2: p2, -2: m2, 3: p3, -3: m3}
    for k in (0, 1, -1, 2, -2, 3, -3, 4):
        block = lax.rem(zl + k + 8, 8)
        rows = normed[:, pl.ds(pl.multiple_of(block * 256, 256), 256)]
        weight = far if k == 4 else blocks[k][0:256, :]
        acc = acc + jnp.dot(rows, weight, preferred_element_type=F32)
    query = (acc[:, 0:256] * sq[...]).astype(BF16).astype(F32)
    key = (acc[:, 256:512] * sk[...]).astype(BF16).astype(F32)
    value = (acc[:, 512:768] * sv[...]).astype(BF16).astype(F32)
    cos = cosine[...]
    sin = sine[...]
    distance = lax.broadcasted_iota(jnp.int32, (LEN, LEN), 0) - lax.broadcasted_iota(jnp.int32, (LEN, LEN), 1)
    distance = distance.astype(F32)
    mask = jnp.where(distance >= 0, jnp.exp(decay * jnp.maximum(distance, 0.0)), 0.0)

    def rotate(values):
        first, second = values[:, 0:128], values[:, 128:256]
        return jnp.concatenate([first * cos - second * sin, second * cos + first * sin], axis=1)

    for s in range(2):
        rows = slice(s * LEN, (s + 1) * LEN)
        rot_query = rotate(query[rows])
        rot_key = rotate(key[rows]) * (256**-0.5)
        scores = lax.dot_general(
            rot_query, rot_key, (((1,), (1,)), ((), ())), precision=HIGH, preferred_element_type=F32
        )
        retained = jnp.dot(scores * mask, value[rows], precision=HIGH, preferred_element_type=F32)
        square = jnp.mean(retained * retained, axis=-1, keepdims=True)
        mixed = (retained * (1.0 / jnp.maximum(jnp.sqrt(square), 1.0))).astype(BF16)
        out[rows, :] = mixed


def ffn_kernel(
    stream, first_heads, last_heads, gain, a0, ap, am, b0, bp, bm, b2p, b2m, sg, su, out, own_rows, resid
):
    zl, y, tp = lax.axis_index("zl"), lax.axis_index("y"), lax.axis_index(TP)
    total = jnp.zeros((256, 1), F32)
    for b in range(8):
        head = (first_heads if b < 4 else last_heads)[b % 2, b // 2 % 2]
        rows = stream[:, b * 256 : (b + 1) * 256].astype(F32) + head.astype(F32)
        resid[b] = rows
        total = total + jnp.sum(rows * rows, axis=-1, keepdims=True)
        own_rows[:, b * 256 : (b + 1) * 256] = resid[b, pl.ds(pl.multiple_of(tp * 32, 32), 32), :]
    inverse = lax.rsqrt(total * (1.0 / 2048) + EPS)
    places = {0: ("a", 0), 1: ("a", 1), -1: ("a", 2), 2: ("a", 3), -2: ("a", 4), 3: ("b", 0), -3: ("b", 1), 4: ("b", 2)}

    def shard(k, j, start, stop):
        batch, place = places[k]
        low, high = place * 96 + start, place * 96 + stop
        if j != 2:
            refs = {"a": {0: a0, 1: ap, 3: am}, "b": {0: b0, 1: bp, 3: bm}}
            return refs[batch][j][low:high, :]
        half, base = (240, 288) if batch == "a" else (144, 0)
        first, second = (bp, bm) if batch == "a" else (b2p, b2m)
        if high <= half:
            return first[base + low : base + high, :]
        if low >= half:
            return second[base + low - half : base + high - half, :]
        return jnp.concatenate([first[base + low : base + half, :], second[base : base + high - half, :]], axis=0)

    def turned(values, by_one, by_two):
        values = jnp.where(by_one, pltpu.roll(values, 192, 1), values)
        return jnp.where(by_two, pltpu.roll(values, 128, 1), values)

    acc = jnp.zeros((256, 768), F32)
    order = (0, 1, -1, 2, -2, 3, -3, 4)
    for k in order:
        block = lax.rem(zl + k + 8, 8)
        rows = turned(resid[block] * inverse * gain[block], y % 2 == 1, y >= 2).astype(BF16)
        weight = jnp.concatenate([shard(k, j, 0, 64) for j in range(4)], axis=0)
        acc = acc + jnp.dot(rows, weight, preferred_element_type=F32)
    gate = acc[:, 0:384] * sg[...]
    hidden = (gate / (1.0 + jnp.exp(-gate)) * (acc[:, 384:768] * su[...])).astype(BF16)
    lane = lax.broadcasted_iota(jnp.int32, (16, 384), 1)
    pick = jnp.where((lane >= 352) & (lane <= 354), 1.0, 0.0).astype(BF16)
    for place, k in enumerate(order):
        pieces = []
        for j in range(4):
            piece = shard(k, j, 64, 96)
            pieces += [piece[:, 0:384], piece[:, 384:768]]
        weight = jnp.concatenate(pieces, axis=0)
        across = (((1,), (1,)), ((), ()))
        scale = lax.dot_general(pick, weight, across, preferred_element_type=F32)
        partial = lax.dot_general(hidden, weight, across, preferred_element_type=F32)
        out[:, place * 256 : (place + 1) * 256] = (partial * scale[0:1, :]).astype(BF16)


def gathered_kernel(own, plus, across, minus, first, second):
    x = lax.axis_index("x")
    for offset, ref in enumerate((own, plus, across, minus)):
        place = lax.rem(x + offset, 4)

        @pl.when(place < 2)
        def _():
            first[lax.rem(place, 2)] = ref[...]

        @pl.when(place >= 2)
        def _():
            second[lax.rem(place, 2)] = ref[...]


def finish_kernel(arrived, own_rows, out):
    zl, y = lax.axis_index("zl"), lax.axis_index("y")
    for place, k in enumerate((0, 1, -1, 2, -2, 3, -3, 4)):
        block = lax.rem(zl + k + 8, 8)
        columns = pl.ds(pl.multiple_of(block * 256, 256), 256)
        total = jnp.zeros((32, 256), F32)
        for i in range(8):
            total = total + arrived[i, :, place * 256 : (place + 1) * 256].astype(F32)
        total = jnp.where(y % 2 == 1, pltpu.roll(total, 64, 1), total)
        total = jnp.where(y >= 2, pltpu.roll(total, 128, 1), total)
        out[:, columns] = (own_rows[:, columns] + total).astype(BF16)


def shards(
    stream, gain_mix, w_query, scale_query, w_key, scale_key, w_value, scale_value,
    gain_ffn, w_gate, scale_gate, w_up, scale_up, w_down, scale_down,
):
    hbm = pl.BlockSpec(memory_space=pltpu.HBM)
    qkv, ffn = call(
        pack_kernel,
        (jax.ShapeDtypeStruct((4, 64, 768), BF16), jax.ShapeDtypeStruct((96, 768), BF16)),
        *[
            pltpu.with_memory_space_constraint(array, pltpu.HBM)
            for array in (w_query, w_key, w_value, w_gate, w_up, w_down, scale_down[None])
        ],
        specs=[hbm] * 7,
        scratch=[pltpu.VMEM((64, n), F32) for n in (256, 256, 256, 352, 352, 352)]
        + [pltpu.VMEM((1, 64), F32), pltpu.SemaphoreType.DMA((7,))],
    )

    def rows_of(count):
        return jax.ShapeDtypeStruct((count, 768), BF16)

    fp1, fm1 = shift(ffn, Z, 1), shift(ffn, Z, -1)
    whole = lax.all_to_all(qkv, "y", split_axis=0, concat_axis=0, tiled=True).reshape(256, 768)
    own, own_m = call(first_kernel, (rows_of(352), rows_of(352)), whole, fp1, fm1)
    p1, m1 = shift(own, Z, 1), shift(own_m, Z, -1)
    p2, m2 = shift(p1, Z, 1), shift(m1, Z, -1)
    a0 = call(batch_a_kernel, rows_of(480), ffn, fp1, fm1, p1, m1)
    ap, am = shift(a0, "y", 1), shift(a0, "y", -1)
    p3, m3 = shift(p2[0:304], Z, 1), shift(m2[0:304], Z, -1)
    p4, m4 = shift(p3[0:128], Z, 1), shift(m3[128:256], Z, -1)
    b0, b0_m = call(batch_b_kernel, (rows_of(528), rows_of(528)), p2, m2, p3, m3, ap, am)
    bp, bm = shift(b0, "y", 1), shift(b0_m, "y", -1)
    b2p, b2m = shift(bp[0:144], "y", 1), shift(bm[144:288], "y", -1)

    stream_f = stream.astype(F32)
    square = jnp.mean(stream_f * stream_f, axis=-1, keepdims=True)
    normed = (stream_f * lax.rsqrt(square + EPS) * gain_mix).astype(BF16)
    angle = np.arange(LEN)[:, None] * THETA ** (-(np.arange(128) / 128))
    cosine, sine = jnp.asarray(np.cos(angle), F32), jnp.asarray(np.sin(angle), F32)
    decays = jnp.asarray(np.log(1.0 - 2.0 ** (-5.0 - np.arange(8))), F32)
    mixed = call(
        retention_kernel,
        jax.ShapeDtypeStruct((256, 256), BF16),
        decays, normed, own, p1, m1, p2, m2, p3, m3, p4, m4,
        scale_query[None], scale_key[None], scale_value[None], cosine, sine,
        specs=[SMEM] + [VMEM] * 15,
    )
    heads = [mixed] + [shift(mixed, "x", i) for i in (1, 2, 3)]
    pair = jax.ShapeDtypeStruct((2, 256, 256), BF16)
    first, second = call(gathered_kernel, (pair, pair), *heads)
    first, second = lax.all_gather(first, "c"), lax.all_gather(second, "c")
    wide = lambda scale: jnp.pad(scale, (0, 32))[None]
    partial, own_rows = call(
        ffn_kernel,
        (jax.ShapeDtypeStruct((256, 2048), BF16), jax.ShapeDtypeStruct((32, 2048), F32)),
        stream, first, second, gain_ffn.reshape(8, 1, 256),
        a0, ap, am, b0, bp, bm, b2p, b2m, wide(scale_gate), wide(scale_up),
        scratch=[pltpu.VMEM((8, 256, 256), F32)],
        limit=12,
    )
    arrived = lax.all_to_all(partial.reshape(8, 32, 2048), TP, split_axis=0, concat_axis=0, tiled=True)
    return call(
        finish_kernel, jax.ShapeDtypeStruct((32, 2048), BF16), arrived, own_rows
    )


def solution(mesh):
    torus = Mesh(
        mesh.devices.reshape(mesh.shape["rep"], mesh.shape["fs"] // 4, 4, 4, 2),
        ("zh", "zl", "y", "x", "c"),
    )
    rows, weight, columns = P(("zh", "zl", "y"), None), P(("zl", "y"), TP), P(TP)
    in_specs = (
        rows, P(), weight, columns, weight, columns, weight, columns,
        P(), weight, columns, weight, columns, weight, P(("zl", "y")),
    )
    return jax.shard_map(
        shards, mesh=torus, in_specs=in_specs, out_specs=P(("zh", "zl", "y", "x", "c"), None), check_vma=False
    )
```

profile of v0, /device:TPU:1, one launch (start us, length us, event | category | flops | bytes accessed | tf_op | source)
XLA Modules:
  0.0 148.0 jit_solution(533019696840663104)
XLA Ops:
  0.0 1.9 %shard_map.172 = (bf16[4,64,768]{2,1,0:T(8,128)(2,1)}, bf16[96,768]{1,0:T(8,128)(2,1)S(1)}) custom-call(f32[64,256]{1,0:T(8,128)} %refs_0_.1, f32[64,256]{1,0:T(8,128)} %refs_1_.1, f32[64,256]{1,0:T(8,128)} %refs_2_.1, f32[64,352]{1,0:T(8,128)} %refs_3_.1, f32[64,352]{1,0:T(8,128)} %refs_4_.1, f32[64,352]{1,0:T(8,128)} %refs_5_.1, f32[1,64]{1,0:T(1,128)} %bitcast.17), custom_call_target="tpu_custom_call" | custom-call | tf_op jit(solution)/shard_map/pallas_call | solution.py:30
  1.9 5.0 %all-to-all-start = ((bf16[4,64,768]{2,1,0:T(8,128)(2,1)}), bf16[4,64,768]{2,1,0:T(8,128)(2,1)S(1)}, u32[]{:S(2)}, u32[]{:S(2)}) async-start(bf16[4,64,768]{2,1,0:T(8,128)(2,1)} %get-tuple-element.15), calls=%async_computation | async-start | bytes 786432 | tf_op jit(solution)/shard_map/all_to_all | solution.py:239
  6.9 3.5 %collective-permute-start.1 = (bf16[96,768]{1,0:T(8,128)(2,1)S(1)}, bf16[96,768]{1,0:T(8,128)(2,1)S(1)}, u32[]{:S(2)}, u32[]{:S(2)}) collective-permute-start(bf16[96,768]{1,0:T(8,128)(2,1)S(1)} %get-tuple-element.16.own), channel_id=1, source_target_pairs={{992,0},{0,32},{32,64},{64,96},{96,128},{128,160},{160,192},{192,2... | collective-permute-start | bytes 442376 | tf_op jit(solution)/shard_map/ppermute | solution.py:26
  10.5 16.8 %collective-permute-start = (bf16[96,768]{1,0:T(8,128)(2,1)S(1)}, bf16[96,768]{1,0:T(8,128)(2,1)S(1)}, u32[]{:S(2)}, u32[]{:S(2)}) collective-permute-start(bf16[96,768]{1,0:T(8,128)(2,1)S(1)} %get-tuple-element.16.own), channel_id=1, source_target_pairs={{32,0},{64,32},{96,64},{128,96},{160,128},{192,160},{224,192},{256... | collective-permute-start | bytes 442376 | tf_op jit(solution)/shard_map/ppermute | solution.py:26
  27.3 1.3 collective-permute-done.1.fm1
  28.6 0.8 collective-permute-done.fp1
  29.3 0.0 all-to-all-done
  29.3 0.1 shard_map.173
  29.4 1.9 %collective-permute-start.3 = (bf16[352,768]{1,0:T(8,128)(2,1)S(1)}, bf16[352,768]{1,0:T(8,128)(2,1)S(1)}, u32[]{:S(2)}, u32[]{:S(2)}) collective-permute-start(bf16[352,768]{1,0:T(8,128)(2,1)S(1)} %get-tuple-element.18), channel_id=1, source_target_pairs={{992,0},{0,32},{32,64},{64,96},{96,128},{128,160},{160,192},{192,2... | collective-permute-start | bytes 1622024 | tf_op jit(solution)/shard_map/ppermute | solution.py:26
  31.3 5.5 %collective-permute-start.2 = (bf16[352,768]{1,0:T(8,128)(2,1)S(1)}, bf16[352,768]{1,0:T(8,128)(2,1)S(1)}, u32[]{:S(2)}, u32[]{:S(2)}) collective-permute-start(bf16[352,768]{1,0:T(8,128)(2,1)S(1)} %get-tuple-element.17.own), channel_id=1, source_target_pairs={{32,0},{64,32},{96,64},{128,96},{160,128},{192,160},{224,192},{256... | collective-permute-start | bytes 1622024 | tf_op jit(solution)/shard_map/ppermute | solution.py:26
  36.8 8.9 %collective-permute-done.3.m1 = bf16[352,768]{1,0:T(8,128)(2,1)S(1)} collective-permute-done((bf16[352,768]{1,0:T(8,128)(2,1)S(1)}, bf16[352,768]{1,0:T(8,128)(2,1)S(1)}, u32[]{:S(2)}, u32[]{:S(2)}) %collective-permute-start.3) | collective-permute-done | bytes 540704 | tf_op jit(solution)/shard_map/ppermute | solution.py:26
  45.7 1.9 %collective-permute-start.5 = (bf16[352,768]{1,0:T(8,128)(2,1)S(1)}, bf16[352,768]{1,0:T(8,128)(2,1)S(1)}, u32[]{:S(2)}, u32[]{:S(2)}) collective-permute-start(bf16[352,768]{1,0:T(8,128)(2,1)S(1)} %collective-permute-done.3.m1), channel_id=1, source_target_pairs={{992,0},{0,32},{32,64},{64,96},{96,128},{128,160},{160,192},{192,2... | collective-permute-start | bytes 1622024 | tf_op jit(solution)/shard_map/ppermute | solution.py:26
  47.6 0.0 collective-permute-done.2.p1
  47.7 4.6 %collective-permute-start.4 = (bf16[352,768]{1,0:T(8,128)(2,1)S(1)}, bf16[352,768]{1,0:T(8,128)(2,1)S(1)}, u32[]{:S(2)}, u32[]{:S(2)}) collective-permute-start(bf16[352,768]{1,0:T(8,128)(2,1)S(1)} %collective-permute-done.2.p1), channel_id=1, source_target_pairs={{32,0},{64,32},{96,64},{128,96},{160,128},{192,160},{224,192},{256... | collective-permute-start | bytes 1622024 | tf_op jit(solution)/shard_map/ppermute | solution.py:26
  52.2 0.1 shard_map.176.a0
  52.3 0.0 copy-start
  52.3 2.5 %collective-permute-start.14 = (bf16[480,768]{1,0:T(8,128)(2,1)S(1)}, bf16[480,768]{1,0:T(8,128)(2,1)S(1)}, u32[]{:S(2)}, u32[]{:S(2)}) collective-permute-start(bf16[480,768]{1,0:T(8,128)(2,1)S(1)} %shard_map.176.a0), channel_id=1, source_target_pairs={{24,0},{0,8},{8,16},{16,24},{25,1},{1,9},{9,17},{17,25},{26,2},{2,... | collective-permute-start | bytes 2211848 | tf_op jit(solution)/shard_map/ppermute | solution.py:26
  54.8 4.2 %collective-permute-start.13 = (bf16[480,768]{1,0:T(8,128)(2,1)S(1)}, bf16[480,768]{1,0:T(8,128)(2,1)S(1)}, u32[]{:S(2)}, u32[]{:S(2)}) collective-permute-start(bf16[480,768]{1,0:T(8,128)(2,1)S(1)} %shard_map.176.a0), channel_id=1, source_target_pairs={{8,0},{16,8},{24,16},{0,24},{9,1},{17,9},{25,17},{1,25},{10,2},{18... | collective-permute-start | bytes 2211848 | tf_op jit(solution)/shard_map/ppermute | solution.py:26
  58.9 1.3 collective-permute-done.5.m2
  60.3 1.9 %collective-permute-start.7 = (bf16[304,768]{1,0:T(8,128)(2,1)S(1)}, bf16[304,768]{1,0:T(8,128)(2,1)S(1)}, u32[]{:S(2)}, u32[]{:S(2)}) collective-permute-start(bf16[304,768]{1,0:T(8,128)(2,1)S(1)} %slice.25), channel_id=1, source_target_pairs={{992,0},{0,32},{32,64},{64,96},{96,128},{128,160},{160,192},{192,2... | collective-permute-start | bytes 1400840 | tf_op jit(solution)/shard_map/ppermute | solution.py:26
  62.2 0.0 collective-permute-done.4.p2
  62.3 4.6 %collective-permute-start.6 = (bf16[304,768]{1,0:T(8,128)(2,1)S(1)}, bf16[304,768]{1,0:T(8,128)(2,1)S(1)}, u32[]{:S(2)}, u32[]{:S(2)}) collective-permute-start(bf16[304,768]{1,0:T(8,128)(2,1)S(1)} %slice.24), channel_id=1, source_target_pairs={{32,0},{64,32},{96,64},{128,96},{160,128},{192,160},{224,192},{256... | collective-permute-start | bytes 1400840 | tf_op jit(solution)/shard_map/ppermute | solution.py:26
  66.9 0.3 fusion
  67.2 3.5 %collective-permute-done.14.am = bf16[480,768]{1,0:T(8,128)(2,1)S(1)} collective-permute-done((bf16[480,768]{1,0:T(8,128)(2,1)S(1)}, bf16[480,768]{1,0:T(8,128)(2,1)S(1)}, u32[]{:S(2)}, u32[]{:S(2)}) %collective-permute-start.14) | collective-permute-done | bytes 737312 | tf_op jit(solution)/shard_map/ppermute | solution.py:26
  70.6 0.9 collective-permute-done.13.ap
  71.5 0.9 collective-permute-done.7.m3
  72.4 1.0 collective-permute-done.6.p3
  73.4 0.1 shard_map.177
  73.5 1.9 %collective-permute-start.16 = (bf16[528,768]{1,0:T(8,128)(2,1)S(1)}, bf16[528,768]{1,0:T(8,128)(2,1)S(1)}, u32[]{:S(2)}, u32[]{:S(2)}) collective-permute-start(bf16[528,768]{1,0:T(8,128)(2,1)S(1)} %get-tuple-element.22), channel_id=1, source_target_pairs={{24,0},{0,8},{8,16},{16,24},{25,1},{1,9},{9,17},{17,25},{26,2},{2,... | collective-permute-start | bytes 2433032 | tf_op jit(solution)/shard_map/ppermute | solution.py:26
  75.4 4.6 %collective-permute-start.15 = (bf16[528,768]{1,0:T(8,128)(2,1)S(1)}, bf16[528,768]{1,0:T(8,128)(2,1)S(1)}, u32[]{:S(2)}, u32[]{:S(2)}) collective-permute-start(bf16[528,768]{1,0:T(8,128)(2,1)S(1)} %get-tuple-element.21.b0), channel_id=1, source_target_pairs={{8,0},{16,8},{24,16},{0,24},{9,1},{17,9},{25,17},{1,25},{10,2},{18... | collective-permute-start | bytes 2433032 | tf_op jit(solution)/shard_map/ppermute | solution.py:26
  80.0 1.9 %collective-permute-start.9 = (bf16[128,768]{1,0:T(8,128)(2,1)S(1)}, bf16[128,768]{1,0:T(8,128)(2,1)S(1)}, u32[]{:S(2)}, u32[]{:S(2)}) collective-permute-start(bf16[128,768]{1,0:T(8,128)(2,1)S(1)} %slice.27), channel_id=1, source_target_pairs={{992,0},{0,32},{32,64},{64,96},{96,128},{128,160},{160,192},{192,2... | collective-permute-start | bytes 589832 | tf_op jit(solution)/shard_map/ppermute | solution.py:26
  82.0 0.0 copy-start.1
  82.0 0.0 copy-start.2
  82.0 0.0 copy-start.4
  82.0 0.0 copy-start.5
  82.0 0.0 copy-start.6
  82.0 0.0 copy-start.7
  82.0 5.5 %collective-permute-start.8 = (bf16[128,768]{1,0:T(8,128)(2,1)S(1)}, bf16[128,768]{1,0:T(8,128)(2,1)S(1)}, u32[]{:S(2)}, u32[]{:S(2)}) collective-permute-start(bf16[128,768]{1,0:T(8,128)(2,1)S(1)} %slice.26), channel_id=1, source_target_pairs={{32,0},{64,32},{96,64},{128,96},{160,128},{192,160},{224,192},{256... | collective-permute-start | bytes 589832 | tf_op jit(solution)/shard_map/ppermute | solution.py:26
  87.5 0.3 fusion.2.normed
  87.8 0.9 collective-permute-done.9.m4
  88.7 1.4 collective-permute-done.8.p4
  90.1 0.0 copy-done.5
  90.1 0.0 copy-start.9
  90.1 0.0 copy-start.10
  90.2 2.8 %shard_map.174.own = bf16[256,256]{1,0:T(8,128)(2,1)S(1)} custom-call(f32[8]{0:T(128)S(1)} %copy-done.7, bf16[256,2048]{1,0:T(8,128)(2,1)S(1)} %fusion.2.normed, bf16[352,768]{1,0:T(8,128)(2,1)S(1)} %get-tuple-element.17.own, bf16[352,768]{1,0:T(8,128)(2,1)S(1)} %collective-permute-done.2.p1, bf16[352,768]{1,0:T(8,128)(2,1)S(1)} %collective-permute-done.3.m1, ...), custom_call_target="tpu_custom_call" | custom-call | tf_op jit(solution)/shard_map/pallas_call | solution.py:30
  93.0 3.1 %collective-permute-start.12 = (bf16[256,256]{1,0:T(8,128)(2,1)S(1)}, bf16[256,256]{1,0:T(8,128)(2,1)S(1)}, u32[]{:S(2)}, u32[]{:S(2)}) collective-permute-start(bf16[256,256]{1,0:T(8,128)(2,1)S(1)} %shard_map.174.own), channel_id=1, source_target_pairs={{6,0},{0,2},{2,4},{4,6},{7,1},{1,3},{3,5},{5,7},{14,8},{8,10},{10,... | collective-permute-start | bytes 393224 | tf_op jit(solution)/shard_map/ppermute | solution.py:26
  96.1 4.4 %collective-permute-start.11 = (bf16[256,256]{1,0:T(8,128)(2,1)S(1)}, bf16[256,256]{1,0:T(8,128)(2,1)S(1)}, u32[]{:S(2)}, u32[]{:S(2)}) collective-permute-start(bf16[256,256]{1,0:T(8,128)(2,1)S(1)} %shard_map.174.own), channel_id=1, source_target_pairs={{4,0},{6,2},{0,4},{2,6},{5,1},{7,3},{1,5},{3,7},{12,8},{14,10},{8,... | collective-permute-start | bytes 393224 | tf_op jit(solution)/shard_map/ppermute | solution.py:26
  100.5 3.1 %collective-permute-start.10 = (bf16[256,256]{1,0:T(8,128)(2,1)S(1)}, bf16[256,256]{1,0:T(8,128)(2,1)S(1)}, u32[]{:S(2)}, u32[]{:S(2)}) collective-permute-start(bf16[256,256]{1,0:T(8,128)(2,1)S(1)} %shard_map.174.own), channel_id=1, source_target_pairs={{2,0},{4,2},{6,4},{0,6},{3,1},{5,3},{7,5},{1,7},{10,8},{12,10},{14... | collective-permute-start | bytes 393224 | tf_op jit(solution)/shard_map/ppermute | solution.py:26
  103.6 0.0 collective-permute-done.12.minus
  103.6 0.0 collective-permute-done.11.across
  103.7 2.8 %collective-permute-done.10.plus = bf16[256,256]{1,0:T(8,128)(2,1)S(1)} collective-permute-done((bf16[256,256]{1,0:T(8,128)(2,1)S(1)}, bf16[256,256]{1,0:T(8,128)(2,1)S(1)}, u32[]{:S(2)}, u32[]{:S(2)}) %collective-permute-start.10) | collective-permute-done | bytes 131104 | tf_op jit(solution)/shard_map/ppermute | solution.py:26
  106.5 0.1 shard_map.175
  106.6 0.0 collective-permute-done.16.bm
  106.6 0.0 copy-start.3
  106.6 1.9 %collective-permute-start.18 = (bf16[144,768]{1,0:T(8,128)(2,1)S(1)}, bf16[144,768]{1,0:T(8,128)(2,1)S(1)}, u32[]{:S(2)}, u32[]{:S(2)}) collective-permute-start(bf16[144,768]{1,0:T(8,128)(2,1)S(1)} %slice.29), channel_id=1, source_target_pairs={{24,0},{0,8},{8,16},{16,24},{25,1},{1,9},{9,17},{17,25},{26,2},{2,... | collective-permute-start | bytes 663560 | tf_op jit(solution)/shard_map/ppermute | solution.py:26
  108.5 0.0 collective-permute-done.15.bp
  108.6 4.6 %collective-permute-start.17 = (bf16[144,768]{1,0:T(8,128)(2,1)S(1)}, bf16[144,768]{1,0:T(8,128)(2,1)S(1)}, u32[]{:S(2)}, u32[]{:S(2)}) collective-permute-start(bf16[144,768]{1,0:T(8,128)(2,1)S(1)} %slice.28), channel_id=1, source_target_pairs={{8,0},{16,8},{24,16},{0,24},{9,1},{17,9},{25,17},{1,25},{10,2},{18... | collective-permute-start | bytes 663560 | tf_op jit(solution)/shard_map/ppermute | solution.py:26
  113.2 9.6 %all-gather = bf16[4,256,256]{2,1,0:T(8,128)(2,1)S(1)} all-gather(bf16[2,256,256]{2,1,0:T(8,128)(2,1)S(1)} %get-tuple-element.19), channel_id=2, replica_groups=mesh['zh'=4,'zl'=8,'y'=4,'x'=4,'c'=2] {'c'}, dimensions={0}, use_global_device_ids=true | all-gather | bytes 786432 | tf_op jit(solution)/shard_map/all_gather | solution.py:267
  122.8 2.2 %all-gather.1 = bf16[4,256,256]{2,1,0:T(8,128)(2,1)S(1)} all-gather(bf16[2,256,256]{2,1,0:T(8,128)(2,1)S(1)} %get-tuple-element.20), channel_id=3, replica_groups=mesh['zh'=4,'zl'=8,'y'=4,'x'=4,'c'=2] {'c'}, dimensions={0}, use_global_device_ids=true | all-gather | bytes 786432 | tf_op jit(solution)/shard_map/all_gather | solution.py:267
  124.9 0.0 collective-permute-done.18.b2m
  124.9 0.0 collective-permute-done.17.b2p
  125.0 3.1 %shard_map.178 = (bf16[256,2048]{1,0:T(8,128)(2,1)S(1)}, f32[32,2048]{1,0:T(8,128)S(1)}) custom-call(bf16[256,2048]{1,0:T(8,128)(2,1)S(1)} %copy-done, bf16[2,2,256,256]{3,2,1,0:T(8,128)(2,1)S(1)} %bitcast.9, bf16[2,2,256,256]{3,2,1,0:T(8,128)(2,1)S(1)} %bitcast.10, f32[8,1,256]{2,1,0:T(1,128)S(1)} %bitcast.13, bf16[480,768]{1,0:T(8,128)(2,1)S(1)} %shard_map.176.a0, ...), custom_call_target="tpu_custom_call" | custom-call | tf_op jit(solution)/shard_map/pallas_call | solution.py:30
  128.1 19.0 %all_to_all.10.arrived = bf16[8,32,2048]{2,1,0:T(8,128)(2,1)S(1)} all-to-all(bf16[8,32,2048]{2,1,0:T(8,128)(2,1)S(1)} %bitcast.12), channel_id=1, replica_groups=mesh['zh'=4,'zl'=8,'y'=4,'x'=4,'c'=2] {'x','c'}, dimensions={0} | all-to-all | bytes 2097152 | tf_op jit(solution)/shard_map/all_to_all | solution.py:277
  147.1 0.9 shard_map.179
  (22 shorter events, 0.2 us)
Async XLA Ops:
  1.9 27.4 %all-to-all-start = ((bf16[4,64,768]{2,1,0:T(8,128)(2,1)}), bf16[4,64,768]{2,1,0:T(8,128)(2,1)S(1)}, u32[]{:S(2)}, u32[]{:S(2)}) async-start(bf16[4,64,768]{2,1,0:T(8,128)(2,1)} %get-tuple-element.15), calls=%async_computation | async-start | bytes 786432 | tf_op jit(solution)/shard_map/all_to_all | solution.py:239
  6.9 21.7 %collective-permute-start.1 = (bf16[96,768]{1,0:T(8,128)(2,1)S(1)}, bf16[96,768]{1,0:T(8,128)(2,1)S(1)}, u32[]{:S(2)}, u32[]{:S(2)}) collective-permute-start(bf16[96,768]{1,0:T(8,128)(2,1)S(1)} %get-tuple-element.16.own), channel_id=1, source_target_pairs={{992,0},{0,32},{32,64},{64,96},{96,128},{128,160},{160,192},{192,2... | collective-permute-start | bytes 442376 | tf_op jit(solution)/shard_map/ppermute | solution.py:26
  10.5 18.9 %collective-permute-start = (bf16[96,768]{1,0:T(8,128)(2,1)S(1)}, bf16[96,768]{1,0:T(8,128)(2,1)S(1)}, u32[]{:S(2)}, u32[]{:S(2)}) collective-permute-start(bf16[96,768]{1,0:T(8,128)(2,1)S(1)} %get-tuple-element.16.own), channel_id=1, source_target_pairs={{32,0},{64,32},{96,64},{128,96},{160,128},{192,160},{224,192},{256... | collective-permute-start | bytes 442376 | tf_op jit(solution)/shard_map/ppermute | solution.py:26
  29.4 16.3 %collective-permute-start.3 = (bf16[352,768]{1,0:T(8,128)(2,1)S(1)}, bf16[352,768]{1,0:T(8,128)(2,1)S(1)}, u32[]{:S(2)}, u32[]{:S(2)}) collective-permute-start(bf16[352,768]{1,0:T(8,128)(2,1)S(1)} %get-tuple-element.18), channel_id=1, source_target_pairs={{992,0},{0,32},{32,64},{64,96},{96,128},{128,160},{160,192},{192,2... | collective-permute-start | bytes 1622024 | tf_op jit(solution)/shard_map/ppermute | solution.py:26
  31.3 16.3 %collective-permute-start.2 = (bf16[352,768]{1,0:T(8,128)(2,1)S(1)}, bf16[352,768]{1,0:T(8,128)(2,1)S(1)}, u32[]{:S(2)}, u32[]{:S(2)}) collective-permute-start(bf16[352,768]{1,0:T(8,128)(2,1)S(1)} %get-tuple-element.17.own), channel_id=1, source_target_pairs={{32,0},{64,32},{96,64},{128,96},{160,128},{192,160},{224,192},{256... | collective-permute-start | bytes 1622024 | tf_op jit(solution)/shard_map/ppermute | solution.py:26
  45.7 14.5 %collective-permute-start.5 = (bf16[352,768]{1,0:T(8,128)(2,1)S(1)}, bf16[352,768]{1,0:T(8,128)(2,1)S(1)}, u32[]{:S(2)}, u32[]{:S(2)}) collective-permute-start(bf16[352,768]{1,0:T(8,128)(2,1)S(1)} %collective-permute-done.3.m1), channel_id=1, source_target_pairs={{992,0},{0,32},{32,64},{64,96},{96,128},{128,160},{160,192},{192,2... | collective-permute-start | bytes 1622024 | tf_op jit(solution)/shard_map/ppermute | solution.py:26
  47.7 14.6 %collective-permute-start.4 = (bf16[352,768]{1,0:T(8,128)(2,1)S(1)}, bf16[352,768]{1,0:T(8,128)(2,1)S(1)}, u32[]{:S(2)}, u32[]{:S(2)}) collective-permute-start(bf16[352,768]{1,0:T(8,128)(2,1)S(1)} %collective-permute-done.2.p1), channel_id=1, source_target_pairs={{32,0},{64,32},{96,64},{128,96},{160,128},{192,160},{224,192},{256... | collective-permute-start | bytes 1622024 | tf_op jit(solution)/shard_map/ppermute | solution.py:26
  52.3 14.6 %copy-start = (bf16[256,2048]{1,0:T(8,128)(2,1)S(1)}, bf16[256,2048]{1,0:T(8,128)(2,1)}, u32[]{:S(2)}) copy-start(bf16[256,2048]{1,0:T(8,128)(2,1)} %stream.1) | copy-start | bytes 3145732
  52.3 18.3 %collective-permute-start.14 = (bf16[480,768]{1,0:T(8,128)(2,1)S(1)}, bf16[480,768]{1,0:T(8,128)(2,1)S(1)}, u32[]{:S(2)}, u32[]{:S(2)}) collective-permute-start(bf16[480,768]{1,0:T(8,128)(2,1)S(1)} %shard_map.176.a0), channel_id=1, source_target_pairs={{24,0},{0,8},{8,16},{16,24},{25,1},{1,9},{9,17},{17,25},{26,2},{2,... | collective-permute-start | bytes 2211848 | tf_op jit(solution)/shard_map/ppermute | solution.py:26
  54.8 16.8 %collective-permute-start.13 = (bf16[480,768]{1,0:T(8,128)(2,1)S(1)}, bf16[480,768]{1,0:T(8,128)(2,1)S(1)}, u32[]{:S(2)}, u32[]{:S(2)}) collective-permute-start(bf16[480,768]{1,0:T(8,128)(2,1)S(1)} %shard_map.176.a0), channel_id=1, source_target_pairs={{8,0},{16,8},{24,16},{0,24},{9,1},{17,9},{25,17},{1,25},{10,2},{18... | collective-permute-start | bytes 2211848 | tf_op jit(solution)/shard_map/ppermute | solution.py:26
  60.3 12.1 %collective-permute-start.7 = (bf16[304,768]{1,0:T(8,128)(2,1)S(1)}, bf16[304,768]{1,0:T(8,128)(2,1)S(1)}, u32[]{:S(2)}, u32[]{:S(2)}) collective-permute-start(bf16[304,768]{1,0:T(8,128)(2,1)S(1)} %slice.25), channel_id=1, source_target_pairs={{992,0},{0,32},{32,64},{64,96},{96,128},{128,160},{160,192},{192,2... | collective-permute-start | bytes 1400840 | tf_op jit(solution)/shard_map/ppermute | solution.py:26
  62.3 11.1 %collective-permute-start.6 = (bf16[304,768]{1,0:T(8,128)(2,1)S(1)}, bf16[304,768]{1,0:T(8,128)(2,1)S(1)}, u32[]{:S(2)}, u32[]{:S(2)}) collective-permute-start(bf16[304,768]{1,0:T(8,128)(2,1)S(1)} %slice.24), channel_id=1, source_target_pairs={{32,0},{64,32},{96,64},{128,96},{160,128},{192,160},{224,192},{256... | collective-permute-start | bytes 1400840 | tf_op jit(solution)/shard_map/ppermute | solution.py:26
  67.2 20.4 %copy-start.8 = (f32[2048]{0:T(1024)S(1)}, f32[2048]{0:T(1024)}, u32[]{:S(2)}) copy-start(f32[2048]{0:T(1024)} %param.19) | copy-start | bytes 24580
  73.5 33.1 %collective-permute-start.16 = (bf16[528,768]{1,0:T(8,128)(2,1)S(1)}, bf16[528,768]{1,0:T(8,128)(2,1)S(1)}, u32[]{:S(2)}, u32[]{:S(2)}) collective-permute-start(bf16[528,768]{1,0:T(8,128)(2,1)S(1)} %get-tuple-element.22), channel_id=1, source_target_pairs={{24,0},{0,8},{8,16},{16,24},{25,1},{1,9},{9,17},{17,25},{26,2},{2,... | collective-permute-start | bytes 2433032 | tf_op jit(solution)/shard_map/ppermute | solution.py:26
  75.4 33.1 %collective-permute-start.15 = (bf16[528,768]{1,0:T(8,128)(2,1)S(1)}, bf16[528,768]{1,0:T(8,128)(2,1)S(1)}, u32[]{:S(2)}, u32[]{:S(2)}) collective-permute-start(bf16[528,768]{1,0:T(8,128)(2,1)S(1)} %get-tuple-element.21.b0), channel_id=1, source_target_pairs={{8,0},{16,8},{24,16},{0,24},{9,1},{17,9},{25,17},{1,25},{10,2},{18... | collective-permute-start | bytes 2433032 | tf_op jit(solution)/shard_map/ppermute | solution.py:26
  80.0 8.7 %collective-permute-start.9 = (bf16[128,768]{1,0:T(8,128)(2,1)S(1)}, bf16[128,768]{1,0:T(8,128)(2,1)S(1)}, u32[]{:S(2)}, u32[]{:S(2)}) collective-permute-start(bf16[128,768]{1,0:T(8,128)(2,1)S(1)} %slice.27), channel_id=1, source_target_pairs={{992,0},{0,32},{32,64},{64,96},{96,128},{128,160},{160,192},{192,2... | collective-permute-start | bytes 589832 | tf_op jit(solution)/shard_map/ppermute | solution.py:26
  82.0 8.1 %copy-start.1 = (f32[128,128]{1,0:T(8,128)S(1)}, f32[128,128]{1,0:T(8,128)}, u32[]{:S(2)}) copy-start(f32[128,128]{1,0:T(8,128)} %constant.16.clone.sine) | copy-start | bytes 196612
  82.0 8.1 %copy-start.2 = (f32[128,128]{1,0:T(8,128)S(1)}, f32[128,128]{1,0:T(8,128)}, u32[]{:S(2)}) copy-start(f32[128,128]{1,0:T(8,128)} %constant.15.clone.cosine) | copy-start | bytes 196612
  82.0 8.1 %copy-start.4 = (f32[256]{0:T(256)S(1)}, f32[256]{0:T(256)}, u32[]{:S(2)}) copy-start(f32[256]{0:T(256)} %param.21) | copy-start | bytes 3076
  82.0 8.1 %copy-start.5 = (f32[256]{0:T(256)S(1)}, f32[256]{0:T(256)}, u32[]{:S(2)}) copy-start(f32[256]{0:T(256)} %param.23) | copy-start | bytes 3076
  82.0 8.1 %copy-start.6 = (f32[256]{0:T(256)S(1)}, f32[256]{0:T(256)}, u32[]{:S(2)}) copy-start(f32[256]{0:T(256)} %param.25) | copy-start | bytes 3076
  82.0 8.1 %copy-start.7 = (f32[8]{0:T(128)S(1)}, f32[8]{0:T(128)}, u32[]{:S(2)}) copy-start(f32[8]{0:T(128)} %constant.17.clone.decays) | copy-start | bytes 100
  82.0 8.1 %collective-permute-start.8 = (bf16[128,768]{1,0:T(8,128)(2,1)S(1)}, bf16[128,768]{1,0:T(8,128)(2,1)S(1)}, u32[]{:S(2)}, u32[]{:S(2)}) collective-permute-start(bf16[128,768]{1,0:T(8,128)(2,1)S(1)} %slice.26), channel_id=1, source_target_pairs={{32,0},{64,32},{96,64},{128,96},{160,128},{192,160},{224,192},{256... | collective-permute-start | bytes 589832 | tf_op jit(solution)/shard_map/ppermute | solution.py:26
  90.1 13.4 %copy-start.9 = (f32[352]{0:T(512)S(1)}, f32[352]{0:T(512)}, u32[]{:S(2)}) copy-start(f32[352]{0:T(512)} %param.28) | copy-start | bytes 4228
  90.1 13.5 %copy-start.10 = (f32[352]{0:T(512)S(1)}, f32[352]{0:T(512)}, u32[]{:S(2)}) copy-start(f32[352]{0:T(512)} %param.30) | copy-start | bytes 4228
  93.0 10.6 %collective-permute-start.12 = (bf16[256,256]{1,0:T(8,128)(2,1)S(1)}, bf16[256,256]{1,0:T(8,128)(2,1)S(1)}, u32[]{:S(2)}, u32[]{:S(2)}) collective-permute-start(bf16[256,256]{1,0:T(8,128)(2,1)S(1)} %shard_map.174.own), channel_id=1, source_target_pairs={{6,0},{0,2},{2,4},{4,6},{7,1},{1,3},{3,5},{5,7},{14,8},{8,10},{10,... | collective-permute-start | bytes 393224 | tf_op jit(solution)/shard_map/ppermute | solution.py:26
  96.1 7.5 %collective-permute-start.11 = (bf16[256,256]{1,0:T(8,128)(2,1)S(1)}, bf16[256,256]{1,0:T(8,128)(2,1)S(1)}, u32[]{:S(2)}, u32[]{:S(2)}) collective-permute-start(bf16[256,256]{1,0:T(8,128)(2,1)S(1)} %shard_map.174.own), channel_id=1, source_target_pairs={{4,0},{6,2},{0,4},{2,6},{5,1},{7,3},{1,5},{3,7},{12,8},{14,10},{8,... | collective-permute-start | bytes 393224 | tf_op jit(solution)/shard_map/ppermute | solution.py:26
  100.5 6.0 %collective-permute-start.10 = (bf16[256,256]{1,0:T(8,128)(2,1)S(1)}, bf16[256,256]{1,0:T(8,128)(2,1)S(1)}, u32[]{:S(2)}, u32[]{:S(2)}) collective-permute-start(bf16[256,256]{1,0:T(8,128)(2,1)S(1)} %shard_map.174.own), channel_id=1, source_target_pairs={{2,0},{4,2},{6,4},{0,6},{3,1},{5,3},{7,5},{1,7},{10,8},{12,10},{14... | collective-permute-start | bytes 393224 | tf_op jit(solution)/shard_map/ppermute | solution.py:26
  106.6 18.3 %copy-start.3 = (f32[2048]{0:T(1024)S(1)}, f32[2048]{0:T(1024)}, u32[]{:S(2)}) copy-start(f32[2048]{0:T(1024)} %param.26) | copy-start | bytes 24580
  106.6 18.3 %collective-permute-start.18 = (bf16[144,768]{1,0:T(8,128)(2,1)S(1)}, bf16[144,768]{1,0:T(8,128)(2,1)S(1)}, u32[]{:S(2)}, u32[]{:S(2)}) collective-permute-start(bf16[144,768]{1,0:T(8,128)(2,1)S(1)} %slice.29), channel_id=1, source_target_pairs={{24,0},{0,8},{8,16},{16,24},{25,1},{1,9},{9,17},{17,25},{26,2},{2,... | collective-permute-start | bytes 663560 | tf_op jit(solution)/shard_map/ppermute | solution.py:26
  108.6 16.4 %collective-permute-start.17 = (bf16[144,768]{1,0:T(8,128)(2,1)S(1)}, bf16[144,768]{1,0:T(8,128)(2,1)S(1)}, u32[]{:S(2)}, u32[]{:S(2)}) collective-permute-start(bf16[144,768]{1,0:T(8,128)(2,1)S(1)} %slice.28), channel_id=1, source_target_pairs={{8,0},{16,8},{24,16},{0,24},{9,1},{17,9},{25,17},{1,25},{10,2},{18... | collective-permute-start | bytes 663560 | tf_op jit(solution)/shard_map/ppermute | solution.py:26
where the time goes:
time: 149 us; the launch traced here: 148 us
  starting transfers between devices  83.2 us (56%)
  blocking collectives  30.8 us (21%)
  waiting for transfers between devices  23.6 us (16%)
  Pallas kernels  9.08 us (6%)
    ppermute x19, starting transfers between devices, shift(): return lax.ppermute(array, axis, [((i + offset) % n, i) for i in range(n)])  78.2 us
    ppermute x19, waiting for transfers between devices, shift(): return lax.ppermute(array, axis, [((i + offset) % n, i) for i in range(n)])  23.6 us
    all_to_all x1, blocking collectives, shards(): lax.all_to_all(partial.reshape(8, 32, 2048), TP, split_axis=0, concat_axi...  19 us
    all_gather x2, blocking collectives, shards(): first, second = (lax.all_gather(first, 'c'), lax.all_gather(second, 'c'))  11.8 us
    pallas_call x8, Pallas kernels, call(): pl.pallas_call(kernel, out_shape=out_shape, in_specs=specs or [VMEM] * le...  9.08 us
    all_to_all x1, starting transfers between devices, shards(): lax.all_to_all(qkv, 'y', split_axis=0, concat_axis=0, tiled=True)  5.01 us
  transfers between devices with their start and end apart: 20, of which 11 were waited for; matrix products, arithmetic and copies ran while one was open for 1% of the time, Pallas kernels for 2%

commit v1 on v0

v1 whole, which is shorter than its diff:
```python
import jax
import jax.numpy as jnp
import numpy as np
from jax import lax
from jax.experimental import pallas as pl
from jax.experimental.pallas import tpu as pltpu
from jax.sharding import Mesh
from jax.sharding import PartitionSpec as P


EPS = 1e-06
THETA = 10000.0
HIGH = lax.Precision.HIGHEST
LEN = 128
Z = ("zh", "zl")
TP = ("x", "c")
F32 = jnp.float32
BF16 = jnp.bfloat16
VMEM = pl.BlockSpec(memory_space=pltpu.VMEM)
MIB = 1 << 20


def shift(array, axis, offset):
    n = lax.axis_size(axis)
    return lax.ppermute(array, axis, [((i + offset) % n, i) for i in range(n)])


def call(kernel, out_shape, *args, scratch=(), specs=None, limit=6):
    return pl.pallas_call(
        kernel,
        out_shape=out_shape,
        in_specs=specs or [VMEM] * len(args),
        out_specs=jax.tree.map(lambda _: VMEM, out_shape),
        scratch_shapes=list(scratch),
        compiler_params=pltpu.CompilerParams(vmem_limit_bytes=limit * MIB),
    )(*args)


def pack_kernel(*refs):
    sources, qkv, ffn, held, sems = refs[:7], refs[7], refs[8], refs[9:16], refs[16]
    copies = [pltpu.make_async_copy(sources[i], held[i], sems.at[i]) for i in range(7)]
    for copy in copies:
        copy.start()
    copies[6].wait()
    diagonal = lax.broadcasted_iota(jnp.int32, (64, 64), 0) == lax.broadcasted_iota(jnp.int32, (64, 64), 1)
    scale = jnp.sum(jnp.where(diagonal, held[6][...], 0.0), axis=1, keepdims=True)
    high = scale.astype(BF16).astype(F32)
    middle = (scale - high).astype(BF16).astype(F32)
    low = scale - high - middle
    lane = lax.broadcasted_iota(jnp.int32, (64, 384), 1)
    extra = jnp.where(lane == 352, high, jnp.where(lane == 353, middle, jnp.where(lane == 354, low, 0.0)))
    extra = extra.astype(BF16)
    ffn[0:64, :] = jnp.zeros((64, 768), BF16)
    ffn[64:96, 0:384] = extra[0:32]
    ffn[64:96, 384:768] = extra[32:64]
    for copy in copies[:6]:
        copy.wait()
    wq, wk, wv, wg, wu, wd = held[:6]
    for copy in range(4):
        qkv[copy, :, 0:256] = wq[...].astype(BF16)
        qkv[copy, :, 256:512] = wk[...].astype(BF16)
        qkv[copy, :, 512:768] = wv[...].astype(BF16)
    ffn[0:64, 0:352] = wg[...].astype(BF16)
    ffn[0:64, 384:736] = wu[...].astype(BF16)
    down = wd[...].astype(BF16)
    ffn[64:96, 0:352] = down[0:32]
    ffn[64:96, 384:736] = down[32:64]


def first_plus_kernel(qkv, ffn, out):
    out[0:256, :] = qkv[...]
    out[256:352, :] = ffn[...]


def first_minus_kernel(qkv, ffn, out):
    out[0:256, :] = qkv[...]
    out[256:304, :] = ffn[48:96, :]
    out[304:352, :] = ffn[0:48, :]


def near_rows(out, start, plus, minus):
    out[start : start + 96, :] = plus[256:352, :]
    out[start + 96 : start + 144, :] = minus[304:352, :]
    out[start + 144 : start + 192, :] = minus[256:304, :]


def round_a_kernel(own, fp1, fm1, p1, m1, out):
    out[0:96, :] = own[...]
    out[96:192, :] = fp1[...]
    out[192:288, :] = fm1[...]
    near_rows(out, 288, p1, m1)


def round_b_kernel(p2, m2, out):
    near_rows(out, 0, p2, m2)


def round_c_kernel(p3, m3, bp, bm, ap, am, plus, minus, own):
    for out in (plus, minus, own):
        out[0:48, :] = p3[256:304, :]
        out[48:96, :] = m3[256:304, :]
    plus[96:192, :] = bp[0:96, :]
    minus[96:192, :] = bm[96:192, :]
    plus[192:432, :] = ap[0:240, :]
    minus[192:432, :] = am[240:480, :]


def early_kernel(
    stream, gain_mix, cosine, sine, sq, sk, sv, sg, su, gain_ffn, normed, tables, scales, wide, gain
):
    rows = stream[...].astype(F32)
    square = jnp.mean(rows * rows, axis=-1, keepdims=True)
    normed[...] = (rows * lax.rsqrt(square + EPS) * gain_mix[...]).astype(BF16)
    tables[0] = cosine[...]
    tables[1] = sine[...]
    for i, ref in enumerate((sq, sk, sv)):
        scales[i] = ref[...]
    for i, ref in enumerate((sg, su)):
        wide[i] = jnp.zeros((1, 384), F32)
        wide[i, :, 0:352] = ref[...]
    gain[...] = gain_ffn[...]


def retention_kernel(normed, own, p1, m1, p2, m2, p3, m3, p4, scales, tables, out):
    zl = lax.axis_index("zl")
    head, decay = lax.axis_index(TP), jnp.float32(0.0)
    for h in range(8):
        decay = jnp.where(head == h, jnp.float32(np.log(1.0 - 2.0 ** (-5 - h))), decay)
    acc = jnp.zeros((256, 768), F32)
    blocks = {0: own, 1: p1, -1: m1, 2: p2, -2: m2, 3: p3, -3: m3}
    for k in (0, 1, -1, 2, -2, 3, -3, 4):
        block = lax.rem(zl + k + 8, 8)
        rows = normed[:, pl.ds(pl.multiple_of(block * 256, 256), 256)]
        weight = p4[...] if k == 4 else blocks[k][0:256, :]
        acc = acc + jnp.dot(rows, weight, preferred_element_type=F32)
    query = (acc[:, 0:256] * scales[0]).astype(BF16).astype(F32)
    key = (acc[:, 256:512] * scales[1]).astype(BF16).astype(F32)
    value = (acc[:, 512:768] * scales[2]).astype(BF16).astype(F32)
    cos = tables[0]
    sin = tables[1]
    distance = lax.broadcasted_iota(jnp.int32, (LEN, LEN), 0) - lax.broadcasted_iota(jnp.int32, (LEN, LEN), 1)
    distance = distance.astype(F32)
    mask = jnp.where(distance >= 0, jnp.exp(decay * jnp.maximum(distance, 0.0)), 0.0)

    def rotate(values):
        first, second = values[:, 0:128], values[:, 128:256]
        return jnp.concatenate([first * cos - second * sin, second * cos + first * sin], axis=1)

    for s in range(2):
        rows = slice(s * LEN, (s + 1) * LEN)
        rot_query = rotate(query[rows])
        rot_key = rotate(key[rows]) * (256**-0.5)
        scores = lax.dot_general(
            rot_query, rot_key, (((1,), (1,)), ((), ())), precision=HIGH, preferred_element_type=F32
        )
        retained = jnp.dot(scores * mask, value[rows], precision=HIGH, preferred_element_type=F32)
        square = jnp.mean(retained * retained, axis=-1, keepdims=True)
        mixed = (retained * (1.0 / jnp.maximum(jnp.sqrt(square), 1.0))).astype(BF16)
        out[rows, :] = mixed


def ffn_kernel(
    stream, heads, others, gain, a0, ap, am, b0, bp, bm, c0, cp, cm, d2, wide,
    keep, send, own_rows, resid,
):
    zl, y, tp = lax.axis_index("zl"), lax.axis_index("y"), lax.axis_index(TP)
    odd = lax.axis_index("c") == 1
    total = jnp.zeros((256, 1), F32)
    for b in range(8):
        head = jnp.where(odd == (b % 2 == 1), heads[b // 2].astype(F32), others[b // 2].astype(F32))
        rows = stream[:, b * 256 : (b + 1) * 256].astype(F32) + head
        resid[b] = rows
        total = total + jnp.sum(rows * rows, axis=-1, keepdims=True)
        own_rows[:, b * 256 : (b + 1) * 256] = resid[b, pl.ds(pl.multiple_of(tp * 32, 32), 32), :]
    inverse = lax.rsqrt(total * (1.0 / 2048) + EPS)
    mine = {
        0: [(a0, 0, 96)], 1: [(a0, 96, 96)], -1: [(a0, 192, 96)], 2: [(a0, 288, 96)], -2: [(a0, 384, 96)],
        3: [(b0, 0, 96)], -3: [(b0, 96, 96)], 4: [(c0, 0, 96)],
    }
    across = {
        0: [(cp, 192, 96)], 1: [(cp, 288, 96)], -1: [(cp, 384, 48), (cm, 192, 48)], 2: [(cm, 240, 96)],
        -2: [(cm, 336, 96)], 3: [(cp, 96, 96)], -3: [(cm, 96, 96)], 4: [(d2, 0, 96)],
    }
    plus = {id(a0): ap, id(b0): bp, id(c0): cp}
    minus = {id(a0): am, id(b0): bm, id(c0): cm}

    def shard(k, j, start, stop):
        pieces, base = [], 0
        for ref, low, count in across[k] if j == 2 else mine[k]:
            ref = plus[id(ref)] if j == 1 else minus[id(ref)] if j == 3 else ref
            begin, end = max(start, base), min(stop, base + count)
            if begin < end:
                pieces.append(ref[low + begin - base : low + end - base, :])
            base += count
        return pieces[0] if len(pieces) == 1 else jnp.concatenate(pieces, axis=0)

    def turned(values, by_one, by_two):
        values = jnp.where(by_one, pltpu.roll(values, 192, 1), values)
        return jnp.where(by_two, pltpu.roll(values, 128, 1), values)

    acc = jnp.zeros((256, 768), F32)
    order = (0, 1, -1, 2, -2, 3, -3, 4)
    for k in order:
        block = lax.rem(zl + k + 8, 8)
        rows = turned(resid[block] * inverse * gain[block], y % 2 == 1, y >= 2).astype(BF16)
        weight = jnp.concatenate([shard(k, j, 0, 64) for j in range(4)], axis=0)
        acc = acc + jnp.dot(rows, weight, preferred_element_type=F32)
    gate = acc[:, 0:384] * wide[0]
    hidden = (gate / (1.0 + jnp.exp(-gate)) * (acc[:, 384:768] * wide[1])).astype(BF16)
    lane = lax.broadcasted_iota(jnp.int32, (16, 384), 1)
    pick = jnp.where((lane >= 352) & (lane <= 354), 1.0, 0.0).astype(BF16)
    for place, k in enumerate(order):
        pieces = []
        for j in range(4):
            piece = shard(k, j, 64, 96)
            pieces += [piece[:, 0:384], piece[:, 384:768]]
        weight = jnp.concatenate(pieces, axis=0)
        both = (((1,), (1,)), ((), ()))
        scale = lax.dot_general(pick, weight, both, preferred_element_type=F32)
        partial = lax.dot_general(hidden, weight, both, preferred_element_type=F32) * scale[0:1, :]
        partial = partial.reshape(4, 2, 32, 256)
        north, south = partial[:, 1].reshape(128, 256), partial[:, 0].reshape(128, 256)
        columns = slice(place * 256, (place + 1) * 256)
        send[:, columns] = jnp.where(odd, south, north).astype(BF16)
        keep[:, columns] = jnp.where(odd, north, south)


def pair_kernel(keep, other, out):
    for i in range(4):
        rows = slice(i * 32, (i + 1) * 32)
        out[i] = (keep[rows, :] + other[rows, :].astype(F32)).astype(BF16)


def finish_kernel(arrived, own_rows, out):
    zl, y = lax.axis_index("zl"), lax.axis_index("y")
    for place, k in enumerate((0, 1, -1, 2, -2, 3, -3, 4)):
        block = lax.rem(zl + k + 8, 8)
        columns = pl.ds(pl.multiple_of(block * 256, 256), 256)
        total = jnp.zeros((32, 256), F32)
        for i in range(4):
            total = total + arrived[i, :, place * 256 : (place + 1) * 256].astype(F32)
        total = jnp.where(y % 2 == 1, pltpu.roll(total, 64, 1), total)
        total = jnp.where(y >= 2, pltpu.roll(total, 128, 1), total)
        out[:, columns] = (own_rows[:, columns] + total).astype(BF16)


def shards(
    stream, gain_mix, w_query, scale_query, w_key, scale_key, w_value, scale_value,
    gain_ffn, w_gate, scale_gate, w_up, scale_up, w_down, scale_down,
):
    hbm = pl.BlockSpec(memory_space=pltpu.HBM)
    qkv, ffn = call(
        pack_kernel,
        (jax.ShapeDtypeStruct((4, 64, 768), BF16), jax.ShapeDtypeStruct((96, 768), BF16)),
        *[
            pltpu.with_memory_space_constraint(array, pltpu.HBM)
            for array in (w_query, w_key, w_value, w_gate, w_up, w_down, scale_down[None])
        ],
        specs=[hbm] * 7,
        scratch=[pltpu.VMEM((64, n), F32) for n in (256, 256, 256, 352, 352, 352)]
        + [pltpu.VMEM((1, 64), F32), pltpu.SemaphoreType.DMA((7,))],
    )

    def rows_of(count):
        return jax.ShapeDtypeStruct((count, 768), BF16)

    fp1, fm1 = shift(ffn, Z, 1), shift(ffn, Z, -1)
    whole = lax.all_to_all(qkv, "y", split_axis=0, concat_axis=0, tiled=True).reshape(256, 768)
    own = call(first_plus_kernel, rows_of(352), whole, fp1)
    own_m = call(first_minus_kernel, rows_of(352), whole, fm1)
    p1, m1 = shift(own, Z, 1), shift(own_m, Z, -1)
    p2, m2 = shift(p1, Z, 1), shift(m1, Z, -1)
    angle = np.arange(LEN)[:, None] * THETA ** (-(np.arange(128) / 128))
    normed, tables, scales, wide, gain = call(
        early_kernel,
        tuple(
            jax.ShapeDtypeStruct(shape, kind)
            for shape, kind in (
                ((256, 2048), BF16), ((2, LEN, 128), F32), ((3, 1, 256), F32), ((2, 1, 384), F32), ((8, 1, 256), F32)
            )
        ),
        stream, gain_mix[None], jnp.asarray(np.cos(angle), F32), jnp.asarray(np.sin(angle), F32),
        scale_query[None], scale_key[None], scale_value[None], scale_gate[None], scale_up[None],
        gain_ffn.reshape(8, 1, 256), limit=12,
    )
    a0 = call(round_a_kernel, rows_of(480), ffn, fp1, fm1, p1, m1)
    ap, am = shift(a0, "y", 1), shift(a0, "y", -1)
    p3, m3 = shift(p2[0:304], Z, 1), shift(m2[0:304], Z, -1)
    b0 = call(round_b_kernel, rows_of(192), p2, m2)
    bp, bm = shift(b0, "y", 1), shift(b0, "y", -1)
    p4 = shift(p3[0:256], Z, 1)
    c0, c0_m, last = call(round_c_kernel, (rows_of(432), rows_of(432), rows_of(96)), p3, m3, bp, bm, ap, am)
    cp, cm = shift(c0, "y", 1), shift(c0_m, "y", -1)
    d2 = shift(last, "y", 2)

    mixed = call(
        retention_kernel,
        jax.ShapeDtypeStruct((256, 256), BF16),
        normed, own, p1, m1, p2, m2, p3, m3, p4, scales, tables,
    )
    heads = lax.all_gather(mixed, "x")
    others = shift(heads, "c", 1)
    keep, send, own_rows = call(
        ffn_kernel,
        (
            jax.ShapeDtypeStruct((128, 2048), F32),
            jax.ShapeDtypeStruct((128, 2048), BF16),
            jax.ShapeDtypeStruct((32, 2048), F32),
        ),
        stream, heads, others, gain, a0, ap, am, b0, bp, bm, c0, cp, cm, d2, wide,
        scratch=[pltpu.VMEM((8, 256, 256), F32)],
        limit=12,
    )
    partial = call(pair_kernel, jax.ShapeDtypeStruct((4, 32, 2048), BF16), keep, shift(send, "c", 1))
    arrived = lax.all_to_all(partial, "x", split_axis=0, concat_axis=0, tiled=True)
    return call(
        finish_kernel, jax.ShapeDtypeStruct((32, 2048), BF16), arrived, own_rows
    )


def solution(mesh):
    torus = Mesh(
        mesh.devices.reshape(mesh.shape["rep"], mesh.shape["fs"] // 4, 4, 4, 2),
        ("zh", "zl", "y", "x", "c"),
    )
    rows, weight, columns = P(("zh", "zl", "y"), None), P(("zl", "y"), TP), P(TP)
    in_specs = (
        rows, P(), weight, columns, weight, columns, weight, columns,
        P(), weight, columns, weight, columns, weight, P(("zl", "y")),
    )
    return jax.shard_map(
        shards, mesh=torus, in_specs=in_specs, out_specs=P(("zh", "zl", "y", "x", "c"), None), check_vma=False
    )
```

time: 149 us -> 149 us (level)
  blocking collectives: 30.8 us -> 22.4 us
  waiting for transfers between devices: 23.6 us -> 31.8 us
    ppermute x19 -> x18, waiting for transfers between devices: 23.6 us -> 31.8 us  [shift(): return lax.ppermute(array, axis, [((i + offset) % n, i) for i in range(n)])]
    all_to_all x1, blocking collectives: 19 us -> 11.8 us  [shards(): lax.all_to_all(partial, 'x', split_axis=0, concat_axis=0, tiled=True)]
    all_gather x2 -> x1, blocking collectives: 11.8 us -> 10.5 us  [shards(): heads = lax.all_gather(mixed, 'x')]
    ppermute x19 -> x18, starting transfers between devices: 78.2 us -> 79 us  [shift(): return lax.ppermute(array, axis, [((i + offset) % n, i) for i in range(n)])]
    pallas_call x8 -> x11, Pallas kernels: 9.08 us -> 9.01 us  [call(): pl.pallas_call(kernel, out_shape=out_shape, in_specs=specs or [VMEM] * le...]
  transfers between devices with their start and end apart: 20 -> 19, of which waited for: 11 -> 9; matrix products, arithmetic and copies ran while one was open for 1% -> 0% of each run, Pallas kernels for 2% -> 2%
where the time goes in v1:
time: 149 us; the launch traced here: 148 us
  starting transfers between devices  84 us (56%)
  waiting for transfers between devices  31.8 us (21%)
  blocking collectives  22.4 us (15%)
  Pallas kernels  9.01 us (6%)
    ppermute x18, starting transfers between devices, shift(): return lax.ppermute(array, axis, [((i + offset) % n, i) for i in range(n)])  79 us
    ppermute x18, waiting for transfers between devices, shift(): return lax.ppermute(array, axis, [((i + offset) % n, i) for i in range(n)])  31.8 us
    all_to_all x1, blocking collectives, shards(): lax.all_to_all(partial, 'x', split_axis=0, concat_axis=0, tiled=True)  11.8 us
    all_gather x1, blocking collectives, shards(): heads = lax.all_gather(mixed, 'x')  10.5 us
    pallas_call x11, Pallas kernels, call(): pl.pallas_call(kernel, out_shape=out_shape, in_specs=specs or [VMEM] * le...  9.01 us
    all_to_all x1, starting transfers between devices, shards(): lax.all_to_all(qkv, 'y', split_axis=0, concat_axis=0, tiled=True)  5.01 us
  transfers between devices with their start and end apart: 19, of which 9 were waited for; matrix products, arithmetic and copies ran while one was open for 0% of the time, Pallas kernels for 2%

profile of v1, /device:TPU:1, one launch (start us, length us, event | category | flops | bytes accessed | tf_op | source)
XLA Modules:
  0.0 147.7 jit_solution(16715433840652242310)
XLA Ops:
  0.0 1.9 %shard_map.164 = (bf16[4,64,768]{2,1,0:T(8,128)(2,1)}, bf16[96,768]{1,0:T(8,128)(2,1)S(1)}) custom-call(f32[64,256]{1,0:T(8,128)} %refs_0_.1, f32[64,256]{1,0:T(8,128)} %refs_1_.1, f32[64,256]{1,0:T(8,128)} %refs_2_.1, f32[64,352]{1,0:T(8,128)} %refs_3_.1, f32[64,352]{1,0:T(8,128)} %refs_4_.1, f32[64,352]{1,0:T(8,128)} %refs_5_.1, f32[1,64]{1,0:T(1,128)} %bitcast.17), custom_call_target="tpu_custom_call" | custom-call | tf_op jit(solution)/shard_map/pallas_call | solution.py:29
  1.9 5.0 %all-to-all-start = ((bf16[4,64,768]{2,1,0:T(8,128)(2,1)}), bf16[4,64,768]{2,1,0:T(8,128)(2,1)S(1)}, u32[]{:S(2)}, u32[]{:S(2)}) async-start(bf16[4,64,768]{2,1,0:T(8,128)(2,1)} %get-tuple-element.19), calls=%async_computation | async-start | bytes 786432 | tf_op jit(solution)/shard_map/all_to_all | solution.py:268
  6.9 18.4 %collective-permute-start = (bf16[96,768]{1,0:T(8,128)(2,1)S(1)}, bf16[96,768]{1,0:T(8,128)(2,1)S(1)}, u32[]{:S(2)}, u32[]{:S(2)}) collective-permute-start(bf16[96,768]{1,0:T(8,128)(2,1)S(1)} %get-tuple-element.20.own), channel_id=1, source_target_pairs={{32,0},{64,32},{96,64},{128,96},{160,128},{192,160},{224,192},{256... | collective-permute-start | bytes 442376 | tf_op jit(solution)/shard_map/ppermute | solution.py:25
  25.3 2.1 %collective-permute-done.ffn.fp1 = bf16[96,768]{1,0:T(8,128)(2,1)S(1)} collective-permute-done((bf16[96,768]{1,0:T(8,128)(2,1)S(1)}, bf16[96,768]{1,0:T(8,128)(2,1)S(1)}, u32[]{:S(2)}, u32[]{:S(2)}) %collective-permute-start) | collective-permute-done | bytes 147488 | tf_op jit(solution)/shard_map/ppermute | solution.py:25
  27.4 0.0 all-to-all-done
  27.5 5.5 %collective-permute-start.1 = (bf16[352,768]{1,0:T(8,128)(2,1)S(1)}, bf16[352,768]{1,0:T(8,128)(2,1)S(1)}, u32[]{:S(2)}, u32[]{:S(2)}) collective-permute-start(bf16[352,768]{1,0:T(8,128)(2,1)S(1)} %shard_map.165.own), channel_id=1, source_target_pairs={{32,0},{64,32},{96,64},{128,96},{160,128},{192,160},{224,192},{256... | collective-permute-start | bytes 1622024 | tf_op jit(solution)/shard_map/ppermute | solution.py:25
  32.9 1.9 %collective-permute-start.2 = (bf16[96,768]{1,0:T(8,128)(2,1)S(1)}, bf16[96,768]{1,0:T(8,128)(2,1)S(1)}, u32[]{:S(2)}, u32[]{:S(2)}) collective-permute-start(bf16[96,768]{1,0:T(8,128)(2,1)S(1)} %get-tuple-element.20.own), channel_id=1, source_target_pairs={{992,0},{0,32},{32,64},{64,96},{96,128},{128,160},{160,192},{192,2... | collective-permute-start | bytes 442376 | tf_op jit(solution)/shard_map/ppermute | solution.py:25
  34.9 5.2 %collective-permute-done.2.ffn.fm1 = bf16[96,768]{1,0:T(8,128)(2,1)S(1)} collective-permute-done((bf16[96,768]{1,0:T(8,128)(2,1)S(1)}, bf16[96,768]{1,0:T(8,128)(2,1)S(1)}, u32[]{:S(2)}, u32[]{:S(2)}) %collective-permute-start.2) | collective-permute-done | bytes 147488 | tf_op jit(solution)/shard_map/ppermute | solution.py:25
  40.1 1.9 %collective-permute-start.3 = (bf16[352,768]{1,0:T(8,128)(2,1)S(1)}, bf16[352,768]{1,0:T(8,128)(2,1)S(1)}, u32[]{:S(2)}, u32[]{:S(2)}) collective-permute-start(bf16[352,768]{1,0:T(8,128)(2,1)S(1)} %shard_map.166), channel_id=1, source_target_pairs={{992,0},{0,32},{32,64},{64,96},{96,128},{128,160},{160,192},{192,2... | collective-permute-start | bytes 1622024 | tf_op jit(solution)/shard_map/ppermute | solution.py:25
  42.0 0.7 collective-permute-done.1.p1
  42.7 5.3 %collective-permute-start.4 = (bf16[352,768]{1,0:T(8,128)(2,1)S(1)}, bf16[352,768]{1,0:T(8,128)(2,1)S(1)}, u32[]{:S(2)}, u32[]{:S(2)}) collective-permute-start(bf16[352,768]{1,0:T(8,128)(2,1)S(1)} %collective-permute-done.1.p1), channel_id=1, source_target_pairs={{32,0},{64,32},{96,64},{128,96},{160,128},{192,160},{224,192},{256... | collective-permute-start | bytes 1622024 | tf_op jit(solution)/shard_map/ppermute | solution.py:25
  48.1 5.7 %collective-permute-done.3.m1 = bf16[352,768]{1,0:T(8,128)(2,1)S(1)} collective-permute-done((bf16[352,768]{1,0:T(8,128)(2,1)S(1)}, bf16[352,768]{1,0:T(8,128)(2,1)S(1)}, u32[]{:S(2)}, u32[]{:S(2)}) %collective-permute-start.3) | collective-permute-done | bytes 540704 | tf_op jit(solution)/shard_map/ppermute | solution.py:25
  53.8 3.5 %collective-permute-start.10 = (bf16[480,768]{1,0:T(8,128)(2,1)S(1)}, bf16[480,768]{1,0:T(8,128)(2,1)S(1)}, u32[]{:S(2)}, u32[]{:S(2)}) collective-permute-start(bf16[480,768]{1,0:T(8,128)(2,1)S(1)} %shard_map.168.a0), channel_id=1, source_target_pairs={{8,0},{16,8},{24,16},{0,24},{9,1},{17,9},{25,17},{1,25},{10,2},{18... | collective-permute-start | bytes 2211848 | tf_op jit(solution)/shard_map/ppermute | solution.py:25
  57.4 1.9 %collective-permute-start.5 = (bf16[352,768]{1,0:T(8,128)(2,1)S(1)}, bf16[352,768]{1,0:T(8,128)(2,1)S(1)}, u32[]{:S(2)}, u32[]{:S(2)}) collective-permute-start(bf16[352,768]{1,0:T(8,128)(2,1)S(1)} %collective-permute-done.3.m1), channel_id=1, source_target_pairs={{992,0},{0,32},{32,64},{64,96},{96,128},{128,160},{160,192},{192,2... | collective-permute-start | bytes 1622024 | tf_op jit(solution)/shard_map/ppermute | solution.py:25
  59.3 0.0 collective-permute-done.4.p2
  59.4 4.6 %collective-permute-start.6 = (bf16[304,768]{1,0:T(8,128)(2,1)S(1)}, bf16[304,768]{1,0:T(8,128)(2,1)S(1)}, u32[]{:S(2)}, u32[]{:S(2)}) collective-permute-start(bf16[304,768]{1,0:T(8,128)(2,1)S(1)} %slice.12), channel_id=1, source_target_pairs={{32,0},{64,32},{96,64},{128,96},{160,128},{192,160},{224,192},{256... | collective-permute-start | bytes 1400840 | tf_op jit(solution)/shard_map/ppermute | solution.py:25
  63.9 1.9 %collective-permute-start.11 = (bf16[480,768]{1,0:T(8,128)(2,1)S(1)}, bf16[480,768]{1,0:T(8,128)(2,1)S(1)}, u32[]{:S(2)}, u32[]{:S(2)}) collective-permute-start(bf16[480,768]{1,0:T(8,128)(2,1)S(1)} %shard_map.168.a0), channel_id=1, source_target_pairs={{24,0},{0,8},{8,16},{16,24},{25,1},{1,9},{9,17},{17,25},{26,2},{2,... | collective-permute-start | bytes 2211848 | tf_op jit(solution)/shard_map/ppermute | solution.py:25
  65.9 3.5 %collective-permute-done.5.m2 = bf16[352,768]{1,0:T(8,128)(2,1)S(1)} collective-permute-done((bf16[352,768]{1,0:T(8,128)(2,1)S(1)}, bf16[352,768]{1,0:T(8,128)(2,1)S(1)}, u32[]{:S(2)}, u32[]{:S(2)}) %collective-permute-start.5) | collective-permute-done | bytes 540704 | tf_op jit(solution)/shard_map/ppermute | solution.py:25
  69.4 0.0 copy-start
  69.4 2.1 %collective-permute-start.7 = (bf16[304,768]{1,0:T(8,128)(2,1)S(1)}, bf16[304,768]{1,0:T(8,128)(2,1)S(1)}, u32[]{:S(2)}, u32[]{:S(2)}) collective-permute-start(bf16[304,768]{1,0:T(8,128)(2,1)S(1)} %slice.13), channel_id=1, source_target_pairs={{992,0},{0,32},{32,64},{64,96},{96,128},{128,160},{160,192},{192,2... | collective-permute-start | bytes 1400840 | tf_op jit(solution)/shard_map/ppermute | solution.py:25
  71.5 0.0 collective-permute-done.6.p3
  71.5 0.0 copy-start.8
  71.5 0.0 copy-start.1
  71.5 0.0 copy-start.2
  71.6 4.7 %collective-permute-start.8 = (bf16[256,768]{1,0:T(8,128)(2,1)S(1)}, bf16[256,768]{1,0:T(8,128)(2,1)S(1)}, u32[]{:S(2)}, u32[]{:S(2)}) collective-permute-start(bf16[256,768]{1,0:T(8,128)(2,1)S(1)} %slice.14), channel_id=1, source_target_pairs={{32,0},{64,32},{96,64},{128,96},{160,128},{192,160},{224,192},{256... | collective-permute-start | bytes 1179656 | tf_op jit(solution)/shard_map/ppermute | solution.py:25
  76.3 0.0 copy-start.9
  76.3 0.0 copy-start.5
  76.3 0.0 copy-start.6
  76.3 0.0 copy-start.7
  76.3 0.0 copy-start.3
  76.4 0.0 copy-start.4
  76.4 2.5 %collective-permute-start.12 = (bf16[192,768]{1,0:T(8,128)(2,1)S(1)}, bf16[192,768]{1,0:T(8,128)(2,1)S(1)}, u32[]{:S(2)}, u32[]{:S(2)}) collective-permute-start(bf16[192,768]{1,0:T(8,128)(2,1)S(1)} %shard_map.169.b0), channel_id=1, source_target_pairs={{8,0},{16,8},{24,16},{0,24},{9,1},{17,9},{25,17},{1,25},{10,2},{18... | collective-permute-start | bytes 884744 | tf_op jit(solution)/shard_map/ppermute | solution.py:25
  78.9 0.0 collective-permute-done.10.ap
  78.9 2.8 %collective-permute-start.13 = (bf16[192,768]{1,0:T(8,128)(2,1)S(1)}, bf16[192,768]{1,0:T(8,128)(2,1)S(1)}, u32[]{:S(2)}, u32[]{:S(2)}) collective-permute-start(bf16[192,768]{1,0:T(8,128)(2,1)S(1)} %shard_map.169.b0), channel_id=1, source_target_pairs={{24,0},{0,8},{8,16},{16,24},{25,1},{1,9},{9,17},{17,25},{26,2},{2,... | collective-permute-start | bytes 884744 | tf_op jit(solution)/shard_map/ppermute | solution.py:25
  81.7 0.0 copy-done
  81.7 0.0 copy-done.1
  81.7 0.0 copy-done.2
  81.8 0.0 copy-done.5
  81.8 0.0 copy-done.6
  81.8 0.0 copy-done.7
  81.8 0.0 copy-done.3
  81.8 0.4 shard_map.163
  82.2 0.0 collective-permute-done.11.am
  82.2 1.9 %collective-permute-done.12.bp = bf16[192,768]{1,0:T(8,128)(2,1)S(1)} collective-permute-done((bf16[192,768]{1,0:T(8,128)(2,1)S(1)}, bf16[192,768]{1,0:T(8,128)(2,1)S(1)}, u32[]{:S(2)}, u32[]{:S(2)}) %collective-permute-start.12) | collective-permute-done | bytes 294944 | tf_op jit(solution)/shard_map/ppermute | solution.py:25
  84.1 4.3 %collective-permute-done.13.bm = bf16[192,768]{1,0:T(8,128)(2,1)S(1)} collective-permute-done((bf16[192,768]{1,0:T(8,128)(2,1)S(1)}, bf16[192,768]{1,0:T(8,128)(2,1)S(1)}, u32[]{:S(2)}, u32[]{:S(2)}) %collective-permute-start.13) | collective-permute-done | bytes 294944 | tf_op jit(solution)/shard_map/ppermute | solution.py:25
  88.4 0.0 collective-permute-done.7.m3
  88.4 0.1 shard_map.170
  88.5 1.9 %collective-permute-start.14 = (bf16[432,768]{1,0:T(8,128)(2,1)S(1)}, bf16[432,768]{1,0:T(8,128)(2,1)S(1)}, u32[]{:S(2)}, u32[]{:S(2)}) collective-permute-start(bf16[432,768]{1,0:T(8,128)(2,1)S(1)} %get-tuple-element.24.c0), channel_id=1, source_target_pairs={{8,0},{16,8},{24,16},{0,24},{9,1},{17,9},{25,17},{1,25},{10,2},{18... | collective-permute-start | bytes 1990664 | tf_op jit(solution)/shard_map/ppermute | solution.py:25
  90.5 3.4 %collective-permute-start.15 = (bf16[432,768]{1,0:T(8,128)(2,1)S(1)}, bf16[432,768]{1,0:T(8,128)(2,1)S(1)}, u32[]{:S(2)}, u32[]{:S(2)}) collective-permute-start(bf16[432,768]{1,0:T(8,128)(2,1)S(1)} %get-tuple-element.25), channel_id=1, source_target_pairs={{24,0},{0,8},{8,16},{16,24},{25,1},{1,9},{9,17},{17,25},{26,2},{2,... | collective-permute-start | bytes 1990664 | tf_op jit(solution)/shard_map/ppermute | solution.py:25
  93.8 0.0 collective-permute-done.8.p4
  93.8 2.3 %shard_map.167 = bf16[256,256]{1,0:T(8,128)(2,1)S(1)} custom-call(bf16[256,2048]{1,0:T(8,128)(2,1)S(1)} %get-tuple-element.18.normed, bf16[352,768]{1,0:T(8,128)(2,1)S(1)} %shard_map.165.own, bf16[352,768]{1,0:T(8,128)(2,1)S(1)} %collective-permute-done.1.p1, bf16[352,768]{1,0:T(8,128)(2,1)S(1)} %collective-permute-done.3.m1, ...), custom_call_target="tpu_custom_call" | custom-call | tf_op jit(solution)/shard_map/pallas_call | solution.py:29
  96.1 10.5 %all-gather = bf16[1024,256]{1,0:T(8,128)(2,1)S(1)} all-gather(bf16[256,256]{1,0:T(8,128)(2,1)S(1)} %shard_map.167), channel_id=2, replica_groups=mesh['zh'=4,'zl'=8,'y'=4,'x'=4,'c'=2] {'x'}, dimensions={0}, use_global_device_ids=true | all-gather | bytes 655360 | tf_op jit(solution)/shard_map/all_gather | solution.py:301
  106.7 12.0 %collective-permute-start.9 = (bf16[4,256,256]{2,1,0:T(8,128)(2,1)S(1)}, bf16[4,256,256]{2,1,0:T(8,128)(2,1)S(1)}, u32[]{:S(2)}, u32[]{:S(2)}) collective-permute-start(bf16[4,256,256]{2,1,0:T(8,128)(2,1)S(1)} %bitcast.10), channel_id=1, source_target_pairs={{1,0},{0,1},{3,2},{2,3},{5,4},{4,5},{7,6},{6,7},{9,8},{8,9},{11,10... | collective-permute-start | bytes 1572872 | tf_op jit(solution)/shard_map/ppermute | solution.py:25
  118.7 1.9 %collective-permute-start.16 = (bf16[96,768]{1,0:T(8,128)(2,1)S(1)}, bf16[96,768]{1,0:T(8,128)(2,1)S(1)}, u32[]{:S(2)}, u32[]{:S(2)}) collective-permute-start(bf16[96,768]{1,0:T(8,128)(2,1)S(1)} %get-tuple-element.26), channel_id=1, source_target_pairs={{16,0},{24,8},{0,16},{8,24},{17,1},{25,9},{1,17},{9,25},{18,2},{26... | collective-permute-start | bytes 442376 | tf_op jit(solution)/shard_map/ppermute | solution.py:25
  120.6 6.9 %collective-permute-done.16.d2 = bf16[96,768]{1,0:T(8,128)(2,1)S(1)} collective-permute-done((bf16[96,768]{1,0:T(8,128)(2,1)S(1)}, bf16[96,768]{1,0:T(8,128)(2,1)S(1)}, u32[]{:S(2)}, u32[]{:S(2)}) %collective-permute-start.16) | collective-permute-done | bytes 147488 | tf_op jit(solution)/shard_map/ppermute | solution.py:25
  127.5 0.0 collective-permute-done.14.cp
  127.5 0.0 collective-permute-done.15.cm
  127.5 0.0 collective-permute-done.9.others
  127.5 3.2 %shard_map.171 = (f32[128,2048]{1,0:T(8,128)S(1)}, bf16[128,2048]{1,0:T(8,128)(2,1)S(1)}, f32[32,2048]{1,0:T(8,128)S(1)}) custom-call(bf16[256,2048]{1,0:T(8,128)(2,1)S(1)} %copy-done, bf16[4,256,256]{2,1,0:T(8,128)(2,1)S(1)} %bitcast.11, bf16[4,256,256]{2,1,0:T(8,128)(2,1)S(1)} %collective-permute-done.9.others, f32[8,1,256]{2,1,0:T(1,128)S(1)} %get-tuple-element.23.gain, ...), custom_call_target="tpu_custom_call" | custom-call | tf_op jit(solution)/shard_map/pallas_call | solution.py:29
  130.7 2.8 %collective-permute-start.17 = (bf16[128,2048]{1,0:T(8,128)(2,1)S(1)}, bf16[128,2048]{1,0:T(8,128)(2,1)S(1)}, u32[]{:S(2)}, u32[]{:S(2)}) collective-permute-start(bf16[128,2048]{1,0:T(8,128)(2,1)S(1)} %get-tuple-element.29), channel_id=1, source_target_pairs={{1,0},{0,1},{3,2},{2,3},{5,4},{4,5},{7,6},{6,7},{9,8},{8,9},{11,10... | collective-permute-start | bytes 1572872 | tf_op jit(solution)/shard_map/ppermute | solution.py:25
  133.5 1.5 %collective-permute-done.17.other = bf16[128,2048]{1,0:T(8,128)(2,1)S(1)} collective-permute-done((bf16[128,2048]{1,0:T(8,128)(2,1)S(1)}, bf16[128,2048]{1,0:T(8,128)(2,1)S(1)}, u32[]{:S(2)}, u32[]{:S(2)}) %collective-permute-start.17) | collective-permute-done | bytes 524320 | tf_op jit(solution)/shard_map/ppermute | solution.py:25
  135.0 0.1 shard_map.172
  135.1 11.8 %all_to_all.10.arrived = bf16[4,32,2048]{2,1,0:T(8,128)(2,1)S(1)} all-to-all(bf16[4,32,2048]{2,1,0:T(8,128)(2,1)S(1)} %shard_map.172), channel_id=1, replica_groups=mesh['zh'=4,'zl'=8,'y'=4,'x'=4,'c'=2] {'x'}, dimensions={0} | all-to-all | bytes 1048576 | tf_op jit(solution)/shard_map/all_to_all | solution.py:315
  146.9 0.8 shard_map.173
  (12 shorter events, 0.2 us)
Async XLA Ops:
  1.9 25.5 %all-to-all-start = ((bf16[4,64,768]{2,1,0:T(8,128)(2,1)}), bf16[4,64,768]{2,1,0:T(8,128)(2,1)S(1)}, u32[]{:S(2)}, u32[]{:S(2)}) async-start(bf16[4,64,768]{2,1,0:T(8,128)(2,1)} %get-tuple-element.19), calls=%async_computation | async-start | bytes 786432 | tf_op jit(solution)/shard_map/all_to_all | solution.py:268
  6.9 20.5 %collective-permute-start = (bf16[96,768]{1,0:T(8,128)(2,1)S(1)}, bf16[96,768]{1,0:T(8,128)(2,1)S(1)}, u32[]{:S(2)}, u32[]{:S(2)}) collective-permute-start(bf16[96,768]{1,0:T(8,128)(2,1)S(1)} %get-tuple-element.20.own), channel_id=1, source_target_pairs={{32,0},{64,32},{96,64},{128,96},{160,128},{192,160},{224,192},{256... | collective-permute-start | bytes 442376 | tf_op jit(solution)/shard_map/ppermute | solution.py:25
  27.5 15.3 %collective-permute-start.1 = (bf16[352,768]{1,0:T(8,128)(2,1)S(1)}, bf16[352,768]{1,0:T(8,128)(2,1)S(1)}, u32[]{:S(2)}, u32[]{:S(2)}) collective-permute-start(bf16[352,768]{1,0:T(8,128)(2,1)S(1)} %shard_map.165.own), channel_id=1, source_target_pairs={{32,0},{64,32},{96,64},{128,96},{160,128},{192,160},{224,192},{256... | collective-permute-start | bytes 1622024 | tf_op jit(solution)/shard_map/ppermute | solution.py:25
  32.9 7.1 %collective-permute-start.2 = (bf16[96,768]{1,0:T(8,128)(2,1)S(1)}, bf16[96,768]{1,0:T(8,128)(2,1)S(1)}, u32[]{:S(2)}, u32[]{:S(2)}) collective-permute-start(bf16[96,768]{1,0:T(8,128)(2,1)S(1)} %get-tuple-element.20.own), channel_id=1, source_target_pairs={{992,0},{0,32},{32,64},{64,96},{96,128},{128,160},{160,192},{192,2... | collective-permute-start | bytes 442376 | tf_op jit(solution)/shard_map/ppermute | solution.py:25
  40.1 13.7 %collective-permute-start.3 = (bf16[352,768]{1,0:T(8,128)(2,1)S(1)}, bf16[352,768]{1,0:T(8,128)(2,1)S(1)}, u32[]{:S(2)}, u32[]{:S(2)}) collective-permute-start(bf16[352,768]{1,0:T(8,128)(2,1)S(1)} %shard_map.166), channel_id=1, source_target_pairs={{992,0},{0,32},{32,64},{64,96},{96,128},{128,160},{160,192},{192,2... | collective-permute-start | bytes 1622024 | tf_op jit(solution)/shard_map/ppermute | solution.py:25
  42.7 16.6 %collective-permute-start.4 = (bf16[352,768]{1,0:T(8,128)(2,1)S(1)}, bf16[352,768]{1,0:T(8,128)(2,1)S(1)}, u32[]{:S(2)}, u32[]{:S(2)}) collective-permute-start(bf16[352,768]{1,0:T(8,128)(2,1)S(1)} %collective-permute-done.1.p1), channel_id=1, source_target_pairs={{32,0},{64,32},{96,64},{128,96},{160,128},{192,160},{224,192},{256... | collective-permute-start | bytes 1622024 | tf_op jit(solution)/shard_map/ppermute | solution.py:25
  53.8 25.0 %collective-permute-start.10 = (bf16[480,768]{1,0:T(8,128)(2,1)S(1)}, bf16[480,768]{1,0:T(8,128)(2,1)S(1)}, u32[]{:S(2)}, u32[]{:S(2)}) collective-permute-start(bf16[480,768]{1,0:T(8,128)(2,1)S(1)} %shard_map.168.a0), channel_id=1, source_target_pairs={{8,0},{16,8},{24,16},{0,24},{9,1},{17,9},{25,17},{1,25},{10,2},{18... | collective-permute-start | bytes 2211848 | tf_op jit(solution)/shard_map/ppermute | solution.py:25
  57.4 12.0 %collective-permute-start.5 = (bf16[352,768]{1,0:T(8,128)(2,1)S(1)}, bf16[352,768]{1,0:T(8,128)(2,1)S(1)}, u32[]{:S(2)}, u32[]{:S(2)}) collective-permute-start(bf16[352,768]{1,0:T(8,128)(2,1)S(1)} %collective-permute-done.3.m1), channel_id=1, source_target_pairs={{992,0},{0,32},{32,64},{64,96},{96,128},{128,160},{160,192},{192,2... | collective-permute-start | bytes 1622024 | tf_op jit(solution)/shard_map/ppermute | solution.py:25
  59.4 12.1 %collective-permute-start.6 = (bf16[304,768]{1,0:T(8,128)(2,1)S(1)}, bf16[304,768]{1,0:T(8,128)(2,1)S(1)}, u32[]{:S(2)}, u32[]{:S(2)}) collective-permute-start(bf16[304,768]{1,0:T(8,128)(2,1)S(1)} %slice.12), channel_id=1, source_target_pairs={{32,0},{64,32},{96,64},{128,96},{160,128},{192,160},{224,192},{256... | collective-permute-start | bytes 1400840 | tf_op jit(solution)/shard_map/ppermute | solution.py:25
  63.9 18.3 %collective-permute-start.11 = (bf16[480,768]{1,0:T(8,128)(2,1)S(1)}, bf16[480,768]{1,0:T(8,128)(2,1)S(1)}, u32[]{:S(2)}, u32[]{:S(2)}) collective-permute-start(bf16[480,768]{1,0:T(8,128)(2,1)S(1)} %shard_map.168.a0), channel_id=1, source_target_pairs={{24,0},{0,8},{8,16},{16,24},{25,1},{1,9},{9,17},{17,25},{26,2},{2,... | collective-permute-start | bytes 2211848 | tf_op jit(solution)/shard_map/ppermute | solution.py:25
  69.4 12.3 %copy-start = (bf16[256,2048]{1,0:T(8,128)(2,1)S(1)}, bf16[256,2048]{1,0:T(8,128)(2,1)}, u32[]{:S(2)}) copy-start(bf16[256,2048]{1,0:T(8,128)(2,1)} %stream.3) | copy-start | bytes 3145732
  69.4 19.0 %collective-permute-start.7 = (bf16[304,768]{1,0:T(8,128)(2,1)S(1)}, bf16[304,768]{1,0:T(8,128)(2,1)S(1)}, u32[]{:S(2)}, u32[]{:S(2)}) collective-permute-start(bf16[304,768]{1,0:T(8,128)(2,1)S(1)} %slice.13), channel_id=1, source_target_pairs={{992,0},{0,32},{32,64},{64,96},{96,128},{128,160},{160,192},{192,2... | collective-permute-start | bytes 1400840 | tf_op jit(solution)/shard_map/ppermute | solution.py:25
  71.5 10.2 %copy-start.8 = (f32[352]{0:T(512)S(1)}, f32[352]{0:T(512)}, u32[]{:S(2)}) copy-start(f32[352]{0:T(512)} %param.27) | copy-start | bytes 4228
  71.5 10.2 %copy-start.1 = (f32[128,128]{1,0:T(8,128)S(1)}, f32[128,128]{1,0:T(8,128)}, u32[]{:S(2)}) copy-start(f32[128,128]{1,0:T(8,128)} %constant.4.clone.cosine) | copy-start | bytes 196612
  71.5 10.2 %copy-start.2 = (f32[128,128]{1,0:T(8,128)S(1)}, f32[128,128]{1,0:T(8,128)}, u32[]{:S(2)}) copy-start(f32[128,128]{1,0:T(8,128)} %constant.5.clone.sine) | copy-start | bytes 196612
  71.6 22.3 %collective-permute-start.8 = (bf16[256,768]{1,0:T(8,128)(2,1)S(1)}, bf16[256,768]{1,0:T(8,128)(2,1)S(1)}, u32[]{:S(2)}, u32[]{:S(2)}) collective-permute-start(bf16[256,768]{1,0:T(8,128)(2,1)S(1)} %slice.14), channel_id=1, source_target_pairs={{32,0},{64,32},{96,64},{128,96},{160,128},{192,160},{224,192},{256... | collective-permute-start | bytes 1179656 | tf_op jit(solution)/shard_map/ppermute | solution.py:25
  76.3 5.4 %copy-start.9 = (f32[352]{0:T(512)S(1)}, f32[352]{0:T(512)}, u32[]{:S(2)}) copy-start(f32[352]{0:T(512)} %param.29) | copy-start | bytes 4228
  76.3 5.5 %copy-start.5 = (f32[256]{0:T(256)S(1)}, f32[256]{0:T(256)}, u32[]{:S(2)}) copy-start(f32[256]{0:T(256)} %param.20) | copy-start | bytes 3076
  76.3 5.5 %copy-start.6 = (f32[256]{0:T(256)S(1)}, f32[256]{0:T(256)}, u32[]{:S(2)}) copy-start(f32[256]{0:T(256)} %param.22) | copy-start | bytes 3076
  76.3 5.5 %copy-start.7 = (f32[256]{0:T(256)S(1)}, f32[256]{0:T(256)}, u32[]{:S(2)}) copy-start(f32[256]{0:T(256)} %param.24) | copy-start | bytes 3076
  76.3 5.4 %copy-start.3 = (f32[2048]{0:T(1024)S(1)}, f32[2048]{0:T(1024)}, u32[]{:S(2)}) copy-start(f32[2048]{0:T(1024)} %param.18) | copy-start | bytes 24580
  76.4 5.4 %copy-start.4 = (f32[2048]{0:T(1024)S(1)}, f32[2048]{0:T(1024)}, u32[]{:S(2)}) copy-start(f32[2048]{0:T(1024)} %param.25) | copy-start | bytes 24580
  76.4 7.8 %collective-permute-start.12 = (bf16[192,768]{1,0:T(8,128)(2,1)S(1)}, bf16[192,768]{1,0:T(8,128)(2,1)S(1)}, u32[]{:S(2)}, u32[]{:S(2)}) collective-permute-start(bf16[192,768]{1,0:T(8,128)(2,1)S(1)} %shard_map.169.b0), channel_id=1, source_target_pairs={{8,0},{16,8},{24,16},{0,24},{9,1},{17,9},{25,17},{1,25},{10,2},{18... | collective-permute-start | bytes 884744 | tf_op jit(solution)/shard_map/ppermute | solution.py:25
  78.9 9.5 %collective-permute-start.13 = (bf16[192,768]{1,0:T(8,128)(2,1)S(1)}, bf16[192,768]{1,0:T(8,128)(2,1)S(1)}, u32[]{:S(2)}, u32[]{:S(2)}) collective-permute-start(bf16[192,768]{1,0:T(8,128)(2,1)S(1)} %shard_map.169.b0), channel_id=1, source_target_pairs={{24,0},{0,8},{8,16},{16,24},{25,1},{1,9},{9,17},{17,25},{26,2},{2,... | collective-permute-start | bytes 884744 | tf_op jit(solution)/shard_map/ppermute | solution.py:25
  88.5 38.9 %collective-permute-start.14 = (bf16[432,768]{1,0:T(8,128)(2,1)S(1)}, bf16[432,768]{1,0:T(8,128)(2,1)S(1)}, u32[]{:S(2)}, u32[]{:S(2)}) collective-permute-start(bf16[432,768]{1,0:T(8,128)(2,1)S(1)} %get-tuple-element.24.c0), channel_id=1, source_target_pairs={{8,0},{16,8},{24,16},{0,24},{9,1},{17,9},{25,17},{1,25},{10,2},{18... | collective-permute-start | bytes 1990664 | tf_op jit(solution)/shard_map/ppermute | solution.py:25
  90.5 37.0 %collective-permute-start.15 = (bf16[432,768]{1,0:T(8,128)(2,1)S(1)}, bf16[432,768]{1,0:T(8,128)(2,1)S(1)}, u32[]{:S(2)}, u32[]{:S(2)}) collective-permute-start(bf16[432,768]{1,0:T(8,128)(2,1)S(1)} %get-tuple-element.25), channel_id=1, source_target_pairs={{24,0},{0,8},{8,16},{16,24},{25,1},{1,9},{9,17},{17,25},{26,2},{2,... | collective-permute-start | bytes 1990664 | tf_op jit(solution)/shard_map/ppermute | solution.py:25
  106.7 20.8 %collective-permute-start.9 = (bf16[4,256,256]{2,1,0:T(8,128)(2,1)S(1)}, bf16[4,256,256]{2,1,0:T(8,128)(2,1)S(1)}, u32[]{:S(2)}, u32[]{:S(2)}) collective-permute-start(bf16[4,256,256]{2,1,0:T(8,128)(2,1)S(1)} %bitcast.10), channel_id=1, source_target_pairs={{1,0},{0,1},{3,2},{2,3},{5,4},{4,5},{7,6},{6,7},{9,8},{8,9},{11,10... | collective-permute-start | bytes 1572872 | tf_op jit(solution)/shard_map/ppermute | solution.py:25
  118.7 8.8 %collective-permute-start.16 = (bf16[96,768]{1,0:T(8,128)(2,1)S(1)}, bf16[96,768]{1,0:T(8,128)(2,1)S(1)}, u32[]{:S(2)}, u32[]{:S(2)}) collective-permute-start(bf16[96,768]{1,0:T(8,128)(2,1)S(1)} %get-tuple-element.26), channel_id=1, source_target_pairs={{16,0},{24,8},{0,16},{8,24},{17,1},{25,9},{1,17},{9,25},{18,2},{26... | collective-permute-start | bytes 442376 | tf_op jit(solution)/shard_map/ppermute | solution.py:25
  130.7 4.3 %collective-permute-start.17 = (bf16[128,2048]{1,0:T(8,128)(2,1)S(1)}, bf16[128,2048]{1,0:T(8,128)(2,1)S(1)}, u32[]{:S(2)}, u32[]{:S(2)}) collective-permute-start(bf16[128,2048]{1,0:T(8,128)(2,1)S(1)} %get-tuple-element.29), channel_id=1, source_target_pairs={{1,0},{0,1},{3,2},{2,3},{5,4},{4,5},{7,6},{6,7},{9,8},{8,9},{11,10... | collective-permute-start | bytes 1572872 | tf_op jit(solution)/shard_map/ppermute | solution.py:25

commit v2 on v1

--- a/solution.py
+++ b/solution.py
@@ -159,70 +159,108 @@
         out[rows, :] = mixed
 
 
-def ffn_kernel(
-    stream, heads, others, gain, a0, ap, am, b0, bp, bm, c0, cp, cm, d2, wide,
-    keep, send, own_rows, resid,
-):
-    zl, y, tp = lax.axis_index("zl"), lax.axis_index("y"), lax.axis_index(TP)
-    odd = lax.axis_index("c") == 1
+NAMES = ("a0", "ap", "am", "b0", "bp", "bm", "c0", "cp", "cm", "d2")
+MINE = {
+    0: [("a", 0, 96)], 1: [("a", 96, 96)], -1: [("a", 192, 96)], 2: [("a", 288, 96)], -2: [("a", 384, 96)],
+    3: [("b", 0, 96)], -3: [("b", 96, 96)], 4: [("c", 0, 96)],
+}
+ACROSS = {
+    0: [("cp", 192, 96)], 1: [("cp", 288, 96)], -1: [("cp", 384, 48), ("cm", 192, 48)], 2: [("cm", 240, 96)],
+    -2: [("cm", 336, 96)], 3: [("cp", 96, 96)], -3: [("cm", 96, 96)], 4: [("d2", 0, 96)],
+}
+
+
+def shard(refs, k, j, start, stop):
+    pieces, base = [], 0
+    for name, low, count in ACROSS[k] if j == 2 else MINE[k]:
+        ref = refs[name if j == 2 else name + {0: "0", 1: "p", 3: "m"}[j]]
+        begin, end = max(start, base), min(stop, base + count)
+        if begin < end:
+            pieces.append(ref[low + begin - base : low + end - base, :])
+        base += count
+    return pieces[0] if len(pieces) == 1 else jnp.concatenate(pieces, axis=0)
+
+
+def half_sums(refs, side, stream, heads, gain, resid, acc):
+    zl, y = lax.axis_index("zl"), lax.axis_index("y")
     total = jnp.zeros((256, 1), F32)
-    for b in range(8):
-        head = jnp.where(odd == (b % 2 == 1), heads[b // 2].astype(F32), others[b // 2].astype(F32))
-        rows = stream[:, b * 256 : (b + 1) * 256].astype(F32) + head
-        resid[b] = rows
+    for i in range(4):
+        columns = pl.ds(pl.multiple_of((2 * i + side) * 256, 256), 256)
+        rows = stream[:, columns].astype(F32) + heads[i].astype(F32)
+        resid[i] = rows
         total = total + jnp.sum(rows * rows, axis=-1, keepdims=True)
-        own_rows[:, b * 256 : (b + 1) * 256] = resid[b, pl.ds(pl.multiple_of(tp * 32, 32), 32), :]
-    inverse = lax.rsqrt(total * (1.0 / 2048) + EPS)
-    mine = {
-        0: [(a0, 0, 96)], 1: [(a0, 96, 96)], -1: [(a0, 192, 96)], 2: [(a0, 288, 96)], -2: [(a0, 384, 96)],
-        3: [(b0, 0, 96)], -3: [(b0, 96, 96)], 4: [(c0, 0, 96)],
-    }
-    across = {
-        0: [(cp, 192, 96)], 1: [(cp, 288, 96)], -1: [(cp, 384, 48), (cm, 192, 48)], 2: [(cm, 240, 96)],
-        -2: [(cm, 336, 96)], 3: [(cp, 96, 96)], -3: [(cm, 96, 96)], 4: [(d2, 0, 96)],
-    }
-    plus = {id(a0): ap, id(b0): bp, id(c0): cp}
-    minus = {id(a0): am, id(b0): bm, id(c0): cm}
-
-    def shard(k, j, start, stop):
-        pieces, base = [], 0
-        for ref, low, count in across[k] if j == 2 else mine[k]:
-            ref = plus[id(ref)] if j == 1 else minus[id(ref)] if j == 3 else ref
-            begin, end = max(start, base), min(stop, base + count)
-            if begin < end:
-                pieces.append(ref[low + begin - base : low + end - base, :])
-            base += count
-        return pieces[0] if len(pieces) == 1 else jnp.concatenate(pieces, axis=0)
-
-    def turned(values, by_one, by_two):
-        values = jnp.where(by_one, pltpu.roll(values, 192, 1), values)
-        return jnp.where(by_two, pltpu.roll(values, 128, 1), values)
-
-    acc = jnp.zeros((256, 768), F32)
-    order = (0, 1, -1, 2, -2, 3, -3, 4)
-    for k in order:
-        block = lax.rem(zl + k + 8, 8)
-        rows = turned(resid[block] * inverse * gain[block], y % 2 == 1, y >= 2).astype(BF16)
-        weight = jnp.concatenate([shard(k, j, 0, 64) for j in range(4)], axis=0)
-        acc = acc + jnp.dot(rows, weight, preferred_element_type=F32)
-    gate = acc[:, 0:384] * wide[0]
-    hidden = (gate / (1.0 + jnp.exp(-gate)) * (acc[:, 384:768] * wide[1])).astype(BF16)
+
+    def add(offsets):
+        result = None
+        for k in offsets:
+            block = lax.rem(zl + k + 8, 8)
+            rows = resid[lax.div(block, 2)] * gain[block]
+            rows = jnp.where(y % 2 == 1, pltpu.roll(rows, 192, 1), rows)
+            rows = jnp.where(y >= 2, pltpu.roll(rows, 128, 1), rows).astype(BF16)
+            weight = jnp.concatenate([shard(refs, k, j, 0, 64) for j in range(4)], axis=0)
+            part = jnp.dot(rows, weight, preferred_element_type=F32)
+            result = part if result is None else result + part
+        acc[...] = result
+
+    even = lax.rem(zl + side, 2) == 0
+
+    @pl.when(even)
+    def _():
+        add((0, 2, -2, 4))
+
+    @pl.when(jnp.logical_not(even))
+    def _():
+        add((1, -1, 3, -3))
+
+    return total
+
+
+def ffn_own_kernel(stream, heads, gain, *rest):
+    refs = dict(zip(NAMES, rest))
+    resid, acc, total = rest[len(NAMES) :]
+    total[...] = half_sums(refs, lax.axis_index("c"), stream, heads, gain, resid, acc)
+
+
+def rows_for(hidden, side):
+    hidden = hidden.reshape(4, 2, 32, hidden.shape[-1])
+    both = [hidden[:, i].reshape(128, hidden.shape[-1]) for i in range(2)]
+    return jnp.where(side == 1, both[1], both[0])
+
+
+def down_sums(refs, hidden, out):
     lane = lax.broadcasted_iota(jnp.int32, (16, 384), 1)
     pick = jnp.where((lane >= 352) & (lane <= 354), 1.0, 0.0).astype(BF16)
-    for place, k in enumerate(order):
+    hidden = jnp.concatenate([hidden, pick], axis=0)
+    for place, k in enumerate((0, 1, -1, 2, -2, 3, -3, 4)):
         pieces = []
         for j in range(4):
-            piece = shard(k, j, 64, 96)
+            piece = shard(refs, k, j, 64, 96)
             pieces += [piece[:, 0:384], piece[:, 384:768]]
         weight = jnp.concatenate(pieces, axis=0)
-        both = (((1,), (1,)), ((), ()))
-        scale = lax.dot_general(pick, weight, both, preferred_element_type=F32)
-        partial = lax.dot_general(hidden, weight, both, preferred_element_type=F32) * scale[0:1, :]
-        partial = partial.reshape(4, 2, 32, 256)
-        north, south = partial[:, 1].reshape(128, 256), partial[:, 0].reshape(128, 256)
-        columns = slice(place * 256, (place + 1) * 256)
-        send[:, columns] = jnp.where(odd, south, north).astype(BF16)
-        keep[:, columns] = jnp.where(odd, north, south)
+        sums = lax.dot_general(hidden, weight, (((1,), (1,)), ((), ())), preferred_element_type=F32)
+        out[:, place * 256 : (place + 1) * 256] = (sums[0:128] * sums[128:129]).astype(out.dtype)
+
+
+def ffn_kernel(stream, heads, gain, own_resid, own_acc, own_total, wide, *rest):
+    refs = dict(zip(NAMES, rest))
+    send, kept, own_rows, resid, acc = rest[len(NAMES) :]
+    c, tp = lax.axis_index("c"), lax.axis_index(TP)
+    total = own_total[...] + half_sums(refs, 1 - c, stream, heads, gain, resid, acc)
+    mine = pl.ds(pl.multiple_of(tp * 32, 32), 32)
+    for i in range(4):
+        for side, ref in ((c, own_resid), (1 - c, resid)):
+            columns = pl.ds(pl.multiple_of((2 * i + side) * 256, 256), 256)
+            own_rows[:, columns] = ref[i, mine, :]
+    inverse = lax.rsqrt(total * (1.0 / 2048) + EPS)
+    sums = (own_acc[...] + acc[...]) * inverse
+    gate = sums[:, 0:384] * wide[0]
+    hidden = gate / (1.0 + jnp.exp(-gate)) * (sums[:, 384:768] * wide[1])
+    kept[...] = rows_for(hidden, c).astype(BF16)
+    down_sums(refs, rows_for(hidden, 1 - c).astype(BF16), send)
+
+
+def down_kernel(hidden, *rest):
+    down_sums(dict(zip(NAMES, rest)), hidden[...], rest[len(NAMES)])
 
 
 def pair_kernel(keep, other, out):
@@ -288,7 +326,7 @@
     p3, m3 = shift(p2[0:304], Z, 1), shift(m2[0:304], Z, -1)
     b0 = call(round_b_kernel, rows_of(192), p2, m2)
     bp, bm = shift(b0, "y", 1), shift(b0, "y", -1)
-    p4 = shift(p3[0:256], Z, 1)
+    p4 = shift(m3[0:256], Z, -1)
     c0, c0_m, last = call(round_c_kernel, (rows_of(432), rows_of(432), rows_of(96)), p3, m3, bp, bm, ap, am)
     cp, cm = shift(c0, "y", 1), shift(c0_m, "y", -1)
     d2 = shift(last, "y", 2)
@@ -298,20 +336,28 @@
         jax.ShapeDtypeStruct((256, 256), BF16),
         normed, own, p1, m1, p2, m2, p3, m3, p4, scales, tables,
     )
-    heads = lax.all_gather(mixed, "x")
+    heads = lax.all_gather(mixed, "x", axis=0)
     others = shift(heads, "c", 1)
-    keep, send, own_rows = call(
+    shards_of_ffn = (a0, ap, am, b0, bp, bm, c0, cp, cm, d2)
+    own_resid, own_acc, own_total = call(
+        ffn_own_kernel,
+        tuple(jax.ShapeDtypeStruct(shape, F32) for shape in ((4, 256, 256), (256, 768), (256, 1))),
+        stream, heads, gain, *shards_of_ffn, limit=12,
+    )
+    send, kept, own_rows = call(
         ffn_kernel,
         (
-            jax.ShapeDtypeStruct((128, 2048), F32),
             jax.ShapeDtypeStruct((128, 2048), BF16),
+            jax.ShapeDtypeStruct((128, 384), BF16),
             jax.ShapeDtypeStruct((32, 2048), F32),
         ),
-        stream, heads, others, gain, a0, ap, am, b0, bp, bm, c0, cp, cm, d2, wide,
-        scratch=[pltpu.VMEM((8, 256, 256), F32)],
+        stream, others, gain, own_resid, own_acc, own_total, wide, *shards_of_ffn,
+        scratch=[pltpu.VMEM((4, 256, 256), F32), pltpu.VMEM((256, 768), F32)],
         limit=12,
     )
-    partial = call(pair_kernel, jax.ShapeDtypeStruct((4, 32, 2048), BF16), keep, shift(send, "c", 1))
+    other = shift(send, "c", 1)
+    keep = call(down_kernel, jax.ShapeDtypeStruct((128, 2048), F32), kept, *shards_of_ffn, limit=12)
+    partial = call(pair_kernel, jax.ShapeDtypeStruct((4, 32, 2048), BF16), keep, other)
     arrived = lax.all_to_all(partial, "x", split_axis=0, concat_axis=0, tiled=True)
     return call(
         finish_kernel, jax.ShapeDtypeStruct((32, 2048), BF16), arrived, own_rows

time: 149 us -> 146 us (0.980)
  starting transfers between devices: 84 us -> 72.9 us
  waiting for transfers between devices: 31.8 us -> 39.1 us
    ppermute x18, starting transfers between devices: 79 us -> 67.9 us  [shift(): return lax.ppermute(array, axis, [((i + offset) % n, i) for i in range(n)])]
    ppermute x18, waiting for transfers between devices: 31.8 us -> 39 us  [shift(): return lax.ppermute(array, axis, [((i + offset) % n, i) for i in range(n)])]
    pallas_call x11 -> x13, Pallas kernels: 9.01 us -> 9.19 us  [call(): pl.pallas_call(kernel, out_shape=out_shape, in_specs=specs or [VMEM] * le...]
  transfers between devices with their start and end apart: 19 -> 19, of which waited for: 9 -> 9; matrix products, arithmetic and copies ran while one was open for 0% -> 0% of each run, Pallas kernels for 2% -> 3%
where the time goes in v2:
time: 146 us; the launch traced here: 145 us
  starting transfers between devices  72.9 us (50%)
  waiting for transfers between devices  39.1 us (27%)
  blocking collectives  23 us (16%)
  Pallas kernels  9.19 us (6%)
    ppermute x18, starting transfers between devices, shift(): return lax.ppermute(array, axis, [((i + offset) % n, i) for i in range(n)])  67.9 us
    ppermute x18, waiting for transfers between devices, shift(): return lax.ppermute(array, axis, [((i + offset) % n, i) for i in range(n)])  39 us
    all_to_all x1, blocking collectives, shards(): lax.all_to_all(partial, 'x', split_axis=0, concat_axis=0, tiled=True)  11.8 us
    all_gather x1, blocking collectives, shards(): heads = lax.all_gather(mixed, 'x', axis=0)  11.1 us
    pallas_call x13, Pallas kernels, call(): pl.pallas_call(kernel, out_shape=out_shape, in_specs=specs or [VMEM] * le...  9.19 us
    all_to_all x1, starting transfers between devices, shards(): lax.all_to_all(qkv, 'y', split_axis=0, concat_axis=0, tiled=True)  5.01 us
  transfers between devices with their start and end apart: 19, of which 9 were waited for; matrix products, arithmetic and copies ran while one was open for 0% of the time, Pallas kernels for 3%

profile of v2, /device:TPU:1, one launch (start us, length us, event | category | flops | bytes accessed | tf_op | source)
XLA Modules:
  0.0 144.8 jit_solution(13814761499786027104)
XLA Ops:
  0.0 1.9 %shard_map.164 = (bf16[4,64,768]{2,1,0:T(8,128)(2,1)}, bf16[96,768]{1,0:T(8,128)(2,1)S(1)}) custom-call(f32[64,256]{1,0:T(8,128)} %refs_0_.1, f32[64,256]{1,0:T(8,128)} %refs_1_.1, f32[64,256]{1,0:T(8,128)} %refs_2_.1, f32[64,352]{1,0:T(8,128)} %refs_3_.1, f32[64,352]{1,0:T(8,128)} %refs_4_.1, f32[64,352]{1,0:T(8,128)} %refs_5_.1, f32[1,64]{1,0:T(1,128)} %bitcast.17), custom_call_target="tpu_custom_call" | custom-call | tf_op jit(solution)/shard_map/pallas_call | solution.py:29
  1.9 5.0 %all-to-all-start = ((bf16[4,64,768]{2,1,0:T(8,128)(2,1)}), bf16[4,64,768]{2,1,0:T(8,128)(2,1)S(1)}, u32[]{:S(2)}, u32[]{:S(2)}) async-start(bf16[4,64,768]{2,1,0:T(8,128)(2,1)} %get-tuple-element.22), calls=%async_computation | async-start | bytes 786432 | tf_op jit(solution)/shard_map/all_to_all | solution.py:306
  6.9 3.5 %collective-permute-start.2 = (bf16[96,768]{1,0:T(8,128)(2,1)S(1)}, bf16[96,768]{1,0:T(8,128)(2,1)S(1)}, u32[]{:S(2)}, u32[]{:S(2)}) collective-permute-start(bf16[96,768]{1,0:T(8,128)(2,1)S(1)} %get-tuple-element.23.own), channel_id=1, source_target_pairs={{992,0},{0,32},{32,64},{64,96},{96,128},{128,160},{160,192},{192,2... | collective-permute-start | bytes 442376 | tf_op jit(solution)/shard_map/ppermute | solution.py:25
  10.5 18.1 %collective-permute-done.2.ffn.fm1 = bf16[96,768]{1,0:T(8,128)(2,1)S(1)} collective-permute-done((bf16[96,768]{1,0:T(8,128)(2,1)S(1)}, bf16[96,768]{1,0:T(8,128)(2,1)S(1)}, u32[]{:S(2)}, u32[]{:S(2)}) %collective-permute-start.2) | collective-permute-done | bytes 147488 | tf_op jit(solution)/shard_map/ppermute | solution.py:25
  28.6 0.0 all-to-all-done
  28.6 1.9 %collective-permute-start.3 = (bf16[352,768]{1,0:T(8,128)(2,1)S(1)}, bf16[352,768]{1,0:T(8,128)(2,1)S(1)}, u32[]{:S(2)}, u32[]{:S(2)}) collective-permute-start(bf16[352,768]{1,0:T(8,128)(2,1)S(1)} %shard_map.166), channel_id=1, source_target_pairs={{992,0},{0,32},{32,64},{64,96},{96,128},{128,160},{160,192},{192,2... | collective-permute-start | bytes 1622024 | tf_op jit(solution)/shard_map/ppermute | solution.py:25
  30.6 4.6 %collective-permute-start = (bf16[96,768]{1,0:T(8,128)(2,1)S(1)}, bf16[96,768]{1,0:T(8,128)(2,1)S(1)}, u32[]{:S(2)}, u32[]{:S(2)}) collective-permute-start(bf16[96,768]{1,0:T(8,128)(2,1)S(1)} %get-tuple-element.23.own), channel_id=1, source_target_pairs={{32,0},{64,32},{96,64},{128,96},{160,128},{192,160},{224,192},{256... | collective-permute-start | bytes 442376 | tf_op jit(solution)/shard_map/ppermute | solution.py:25
  35.1 2.1 %collective-permute-done.ffn.fp1 = bf16[96,768]{1,0:T(8,128)(2,1)S(1)} collective-permute-done((bf16[96,768]{1,0:T(8,128)(2,1)S(1)}, bf16[96,768]{1,0:T(8,128)(2,1)S(1)}, u32[]{:S(2)}, u32[]{:S(2)}) %collective-permute-start) | collective-permute-done | bytes 147488 | tf_op jit(solution)/shard_map/ppermute | solution.py:25
  37.3 5.0 %collective-permute-start.1 = (bf16[352,768]{1,0:T(8,128)(2,1)S(1)}, bf16[352,768]{1,0:T(8,128)(2,1)S(1)}, u32[]{:S(2)}, u32[]{:S(2)}) collective-permute-start(bf16[352,768]{1,0:T(8,128)(2,1)S(1)} %shard_map.165.own), channel_id=1, source_target_pairs={{32,0},{64,32},{96,64},{128,96},{160,128},{192,160},{224,192},{256... | collective-permute-start | bytes 1622024 | tf_op jit(solution)/shard_map/ppermute | solution.py:25
  42.3 1.8 %collective-permute-done.3.m1 = bf16[352,768]{1,0:T(8,128)(2,1)S(1)} collective-permute-done((bf16[352,768]{1,0:T(8,128)(2,1)S(1)}, bf16[352,768]{1,0:T(8,128)(2,1)S(1)}, u32[]{:S(2)}, u32[]{:S(2)}) %collective-permute-start.3) | collective-permute-done | bytes 540704 | tf_op jit(solution)/shard_map/ppermute | solution.py:25
  44.0 1.9 %collective-permute-start.5 = (bf16[352,768]{1,0:T(8,128)(2,1)S(1)}, bf16[352,768]{1,0:T(8,128)(2,1)S(1)}, u32[]{:S(2)}, u32[]{:S(2)}) collective-permute-start(bf16[352,768]{1,0:T(8,128)(2,1)S(1)} %collective-permute-done.3.m1), channel_id=1, source_target_pairs={{992,0},{0,32},{32,64},{64,96},{96,128},{128,160},{160,192},{192,2... | collective-permute-start | bytes 1622024 | tf_op jit(solution)/shard_map/ppermute | solution.py:25
  46.0 5.0 %collective-permute-done.1.p1 = bf16[352,768]{1,0:T(8,128)(2,1)S(1)} collective-permute-done((bf16[352,768]{1,0:T(8,128)(2,1)S(1)}, bf16[352,768]{1,0:T(8,128)(2,1)S(1)}, u32[]{:S(2)}, u32[]{:S(2)}) %collective-permute-start.1) | collective-permute-done | bytes 540704 | tf_op jit(solution)/shard_map/ppermute | solution.py:25
  51.0 2.8 %collective-permute-start.11 = (bf16[480,768]{1,0:T(8,128)(2,1)S(1)}, bf16[480,768]{1,0:T(8,128)(2,1)S(1)}, u32[]{:S(2)}, u32[]{:S(2)}) collective-permute-start(bf16[480,768]{1,0:T(8,128)(2,1)S(1)} %shard_map.168.rest_0_), channel_id=1, source_target_pairs={{24,0},{0,8},{8,16},{16,24},{25,1},{1,9},{9,17},{17,25},{26,2},{2,... | collective-permute-start | bytes 2211848 | tf_op jit(solution)/shard_map/ppermute | solution.py:25
  53.8 5.3 %collective-permute-start.4 = (bf16[352,768]{1,0:T(8,128)(2,1)S(1)}, bf16[352,768]{1,0:T(8,128)(2,1)S(1)}, u32[]{:S(2)}, u32[]{:S(2)}) collective-permute-start(bf16[352,768]{1,0:T(8,128)(2,1)S(1)} %collective-permute-done.1.p1), channel_id=1, source_target_pairs={{32,0},{64,32},{96,64},{128,96},{160,128},{192,160},{224,192},{256... | collective-permute-start | bytes 1622024 | tf_op jit(solution)/shard_map/ppermute | solution.py:25
  59.1 0.0 collective-permute-done.5.m2
  59.2 1.9 %collective-permute-start.7 = (bf16[304,768]{1,0:T(8,128)(2,1)S(1)}, bf16[304,768]{1,0:T(8,128)(2,1)S(1)}, u32[]{:S(2)}, u32[]{:S(2)}) collective-permute-start(bf16[304,768]{1,0:T(8,128)(2,1)S(1)} %slice.13), channel_id=1, source_target_pairs={{992,0},{0,32},{32,64},{64,96},{96,128},{128,160},{160,192},{192,2... | collective-permute-start | bytes 1400840 | tf_op jit(solution)/shard_map/ppermute | solution.py:25
  61.1 3.7 %collective-permute-start.10 = (bf16[480,768]{1,0:T(8,128)(2,1)S(1)}, bf16[480,768]{1,0:T(8,128)(2,1)S(1)}, u32[]{:S(2)}, u32[]{:S(2)}) collective-permute-start(bf16[480,768]{1,0:T(8,128)(2,1)S(1)} %shard_map.168.rest_0_), channel_id=1, source_target_pairs={{8,0},{16,8},{24,16},{0,24},{9,1},{17,9},{25,17},{1,25},{10,2},{18... | collective-permute-start | bytes 2211848 | tf_op jit(solution)/shard_map/ppermute | solution.py:25
  64.8 1.6 %collective-permute-done.4.p2 = bf16[352,768]{1,0:T(8,128)(2,1)S(1)} collective-permute-done((bf16[352,768]{1,0:T(8,128)(2,1)S(1)}, bf16[352,768]{1,0:T(8,128)(2,1)S(1)}, u32[]{:S(2)}, u32[]{:S(2)}) %collective-permute-start.4) | collective-permute-done | bytes 540704 | tf_op jit(solution)/shard_map/ppermute | solution.py:25
  66.4 0.0 copy-start
  66.4 5.5 %collective-permute-start.6 = (bf16[304,768]{1,0:T(8,128)(2,1)S(1)}, bf16[304,768]{1,0:T(8,128)(2,1)S(1)}, u32[]{:S(2)}, u32[]{:S(2)}) collective-permute-start(bf16[304,768]{1,0:T(8,128)(2,1)S(1)} %slice.12), channel_id=1, source_target_pairs={{32,0},{64,32},{96,64},{128,96},{160,128},{192,160},{224,192},{256... | collective-permute-start | bytes 1400840 | tf_op jit(solution)/shard_map/ppermute | solution.py:25
  71.9 0.0 collective-permute-done.7.m3
  71.9 0.0 copy-start.8
  71.9 0.0 copy-start.1
  71.9 0.0 copy-start.2
  72.0 2.1 %collective-permute-start.8 = (bf16[256,768]{1,0:T(8,128)(2,1)S(1)}, bf16[256,768]{1,0:T(8,128)(2,1)S(1)}, u32[]{:S(2)}, u32[]{:S(2)}) collective-permute-start(bf16[256,768]{1,0:T(8,128)(2,1)S(1)} %slice.14), channel_id=1, source_target_pairs={{992,0},{0,32},{32,64},{64,96},{96,128},{128,160},{160,192},{192,2... | collective-permute-start | bytes 1179656 | tf_op jit(solution)/shard_map/ppermute | solution.py:25
  74.0 0.0 copy-start.9
  74.0 0.0 copy-start.5
  74.0 0.0 copy-start.6
  74.1 0.0 copy-start.7
  74.1 0.0 copy-start.3
  74.1 0.0 copy-start.4
  74.1 3.1 %collective-permute-start.13 = (bf16[192,768]{1,0:T(8,128)(2,1)S(1)}, bf16[192,768]{1,0:T(8,128)(2,1)S(1)}, u32[]{:S(2)}, u32[]{:S(2)}) collective-permute-start(bf16[192,768]{1,0:T(8,128)(2,1)S(1)} %shard_map.169.rest_3_), channel_id=1, source_target_pairs={{24,0},{0,8},{8,16},{16,24},{25,1},{1,9},{9,17},{17,25},{26,2},{2,... | collective-permute-start | bytes 884744 | tf_op jit(solution)/shard_map/ppermute | solution.py:25
  77.2 0.0 collective-permute-done.11.am.rest_2_
  77.2 3.4 %collective-permute-start.12 = (bf16[192,768]{1,0:T(8,128)(2,1)S(1)}, bf16[192,768]{1,0:T(8,128)(2,1)S(1)}, u32[]{:S(2)}, u32[]{:S(2)}) collective-permute-start(bf16[192,768]{1,0:T(8,128)(2,1)S(1)} %shard_map.169.rest_3_), channel_id=1, source_target_pairs={{8,0},{16,8},{24,16},{0,24},{9,1},{17,9},{25,17},{1,25},{10,2},{18... | collective-permute-start | bytes 884744 | tf_op jit(solution)/shard_map/ppermute | solution.py:25
  80.6 0.0 copy-done.8
  80.7 0.0 copy-done.9
  80.7 0.0 copy-done
  80.7 0.0 copy-done.1
  80.7 0.0 copy-done.2
  80.8 0.4 shard_map.163
  81.2 0.0 collective-permute-done.10.ap.rest_1_
  81.2 1.6 %collective-permute-done.13.bm.rest_5_ = bf16[192,768]{1,0:T(8,128)(2,1)S(1)} collective-permute-done((bf16[192,768]{1,0:T(8,128)(2,1)S(1)}, bf16[192,768]{1,0:T(8,128)(2,1)S(1)}, u32[]{:S(2)}, u32[]{:S(2)}) %collective-permute-start.13) | collective-permute-done | bytes 294944 | tf_op jit(solution)/shard_map/ppermute | solution.py:25
  82.8 2.2 %collective-permute-done.12.bp.rest_4_ = bf16[192,768]{1,0:T(8,128)(2,1)S(1)} collective-permute-done((bf16[192,768]{1,0:T(8,128)(2,1)S(1)}, bf16[192,768]{1,0:T(8,128)(2,1)S(1)}, u32[]{:S(2)}, u32[]{:S(2)}) %collective-permute-start.12) | collective-permute-done | bytes 294944 | tf_op jit(solution)/shard_map/ppermute | solution.py:25
  85.0 0.0 collective-permute-done.6.p3
  85.0 0.1 shard_map.170
  85.1 2.8 %collective-permute-start.15 = (bf16[432,768]{1,0:T(8,128)(2,1)S(1)}, bf16[432,768]{1,0:T(8,128)(2,1)S(1)}, u32[]{:S(2)}, u32[]{:S(2)}) collective-permute-start(bf16[432,768]{1,0:T(8,128)(2,1)S(1)} %get-tuple-element.28), channel_id=1, source_target_pairs={{24,0},{0,8},{8,16},{16,24},{25,1},{1,9},{9,17},{17,25},{26,2},{2,... | collective-permute-start | bytes 1990664 | tf_op jit(solution)/shard_map/ppermute | solution.py:25
  87.9 3.7 %collective-permute-start.14 = (bf16[432,768]{1,0:T(8,128)(2,1)S(1)}, bf16[432,768]{1,0:T(8,128)(2,1)S(1)}, u32[]{:S(2)}, u32[]{:S(2)}) collective-permute-start(bf16[432,768]{1,0:T(8,128)(2,1)S(1)} %get-tuple-element.27.rest_6_), channel_id=1, source_target_pairs={{8,0},{16,8},{24,16},{0,24},{9,1},{17,9},{25,17},{1,25},{10,2},{18... | collective-permute-start | bytes 1990664 | tf_op jit(solution)/shard_map/ppermute | solution.py:25
  91.6 0.0 collective-permute-done.8.p4
  91.7 2.3 %shard_map.167 = bf16[256,256]{1,0:T(8,128)(2,1)S(1)} custom-call(bf16[256,2048]{1,0:T(8,128)(2,1)S(1)} %get-tuple-element.21.normed, bf16[352,768]{1,0:T(8,128)(2,1)S(1)} %shard_map.165.own, bf16[352,768]{1,0:T(8,128)(2,1)S(1)} %collective-permute-done.1.p1, bf16[352,768]{1,0:T(8,128)(2,1)S(1)} %collective-permute-done.3.m1, ...), custom_call_target="tpu_custom_call" | custom-call | tf_op jit(solution)/shard_map/pallas_call | solution.py:29
  94.0 11.1 %all-gather = bf16[1024,256]{1,0:T(8,128)(2,1)S(1)} all-gather(bf16[256,256]{1,0:T(8,128)(2,1)S(1)} %shard_map.167), channel_id=2, replica_groups=mesh['zh'=4,'zl'=8,'y'=4,'x'=4,'c'=2] {'x'}, dimensions={0}, use_global_device_ids=true | all-gather | bytes 655360 | tf_op jit(solution)/shard_map/all_gather | solution.py:339
  105.1 11.1 %collective-permute-start.9 = (bf16[4,256,256]{2,1,0:T(8,128)(2,1)S(1)}, bf16[4,256,256]{2,1,0:T(8,128)(2,1)S(1)}, u32[]{:S(2)}, u32[]{:S(2)}) collective-permute-start(bf16[4,256,256]{2,1,0:T(8,128)(2,1)S(1)} %bitcast.10), channel_id=1, source_target_pairs={{1,0},{0,1},{3,2},{2,3},{5,4},{4,5},{7,6},{6,7},{9,8},{8,9},{11,10... | collective-permute-start | bytes 1572872 | tf_op jit(solution)/shard_map/ppermute | solution.py:25
  116.2 2.9 %collective-permute-start.16 = (bf16[96,768]{1,0:T(8,128)(2,1)S(1)}, bf16[96,768]{1,0:T(8,128)(2,1)S(1)}, u32[]{:S(2)}, u32[]{:S(2)}) collective-permute-start(bf16[96,768]{1,0:T(8,128)(2,1)S(1)} %get-tuple-element.29), channel_id=1, source_target_pairs={{16,0},{24,8},{0,16},{8,24},{17,1},{25,9},{1,17},{9,25},{18,2},{26... | collective-permute-start | bytes 442376 | tf_op jit(solution)/shard_map/ppermute | solution.py:25
  119.0 5.9 %collective-permute-done.16.rest_9_ = bf16[96,768]{1,0:T(8,128)(2,1)S(1)} collective-permute-done((bf16[96,768]{1,0:T(8,128)(2,1)S(1)}, bf16[96,768]{1,0:T(8,128)(2,1)S(1)}, u32[]{:S(2)}, u32[]{:S(2)}) %collective-permute-start.16) | collective-permute-done | bytes 147488 | tf_op jit(solution)/shard_map/ppermute | solution.py:25
  125.0 0.0 collective-permute-done.15.rest_8_
  125.0 0.0 collective-permute-done.14.rest_7_
  125.0 0.9 shard_map.171
  125.9 0.0 collective-permute-done.9.heads
  125.9 1.8 %shard_map.172 = (bf16[128,2048]{1,0:T(8,128)(2,1)S(1)}, bf16[128,384]{1,0:T(8,128)(2,1)S(1)}, f32[32,2048]{1,0:T(8,128)S(1)}) custom-call(bf16[256,2048]{1,0:T(8,128)(2,1)S(1)} %copy-done, bf16[4,256,256]{2,1,0:T(8,128)(2,1)S(1)} %collective-permute-done.9.heads, f32[8,1,256]{2,1,0:T(1,128)S(1)} %get-tuple-element.26.gain, ...), custom_call_target="tpu_custom_call" | custom-call | tf_op jit(solution)/shard_map/pallas_call | solution.py:29
  127.7 2.8 %collective-permute-start.17 = (bf16[128,2048]{1,0:T(8,128)(2,1)S(1)}, bf16[128,2048]{1,0:T(8,128)(2,1)S(1)}, u32[]{:S(2)}, u32[]{:S(2)}) collective-permute-start(bf16[128,2048]{1,0:T(8,128)(2,1)S(1)} %get-tuple-element.35), channel_id=1, source_target_pairs={{1,0},{0,1},{3,2},{2,3},{5,4},{4,5},{7,6},{6,7},{9,8},{8,9},{11,10... | collective-permute-start | bytes 1572872 | tf_op jit(solution)/shard_map/ppermute | solution.py:25
  130.5 0.7 shard_map.173.keep
  131.2 0.8 collective-permute-done.17.other
  132.0 0.1 shard_map.174
  132.1 11.8 %all_to_all.10.arrived = bf16[4,32,2048]{2,1,0:T(8,128)(2,1)S(1)} all-to-all(bf16[4,32,2048]{2,1,0:T(8,128)(2,1)S(1)} %shard_map.174), channel_id=1, replica_groups=mesh['zh'=4,'zl'=8,'y'=4,'x'=4,'c'=2] {'x'}, dimensions={0} | all-to-all | bytes 1048576 | tf_op jit(solution)/shard_map/all_to_all | solution.py:361
  144.0 0.8 shard_map.175
  (14 shorter events, 0.2 us)
Async XLA Ops:
  1.9 26.7 %all-to-all-start = ((bf16[4,64,768]{2,1,0:T(8,128)(2,1)}), bf16[4,64,768]{2,1,0:T(8,128)(2,1)S(1)}, u32[]{:S(2)}, u32[]{:S(2)}) async-start(bf16[4,64,768]{2,1,0:T(8,128)(2,1)} %get-tuple-element.22), calls=%async_computation | async-start | bytes 786432 | tf_op jit(solution)/shard_map/all_to_all | solution.py:306
  6.9 21.7 %collective-permute-start.2 = (bf16[96,768]{1,0:T(8,128)(2,1)S(1)}, bf16[96,768]{1,0:T(8,128)(2,1)S(1)}, u32[]{:S(2)}, u32[]{:S(2)}) collective-permute-start(bf16[96,768]{1,0:T(8,128)(2,1)S(1)} %get-tuple-element.23.own), channel_id=1, source_target_pairs={{992,0},{0,32},{32,64},{64,96},{96,128},{128,160},{160,192},{192,2... | collective-permute-start | bytes 442376 | tf_op jit(solution)/shard_map/ppermute | solution.py:25
  28.6 15.4 %collective-permute-start.3 = (bf16[352,768]{1,0:T(8,128)(2,1)S(1)}, bf16[352,768]{1,0:T(8,128)(2,1)S(1)}, u32[]{:S(2)}, u32[]{:S(2)}) collective-permute-start(bf16[352,768]{1,0:T(8,128)(2,1)S(1)} %shard_map.166), channel_id=1, source_target_pairs={{992,0},{0,32},{32,64},{64,96},{96,128},{128,160},{160,192},{192,2... | collective-permute-start | bytes 1622024 | tf_op jit(solution)/shard_map/ppermute | solution.py:25
  30.6 6.7 %collective-permute-start = (bf16[96,768]{1,0:T(8,128)(2,1)S(1)}, bf16[96,768]{1,0:T(8,128)(2,1)S(1)}, u32[]{:S(2)}, u32[]{:S(2)}) collective-permute-start(bf16[96,768]{1,0:T(8,128)(2,1)S(1)} %get-tuple-element.23.own), channel_id=1, source_target_pairs={{32,0},{64,32},{96,64},{128,96},{160,128},{192,160},{224,192},{256... | collective-permute-start | bytes 442376 | tf_op jit(solution)/shard_map/ppermute | solution.py:25
  37.3 13.7 %collective-permute-start.1 = (bf16[352,768]{1,0:T(8,128)(2,1)S(1)}, bf16[352,768]{1,0:T(8,128)(2,1)S(1)}, u32[]{:S(2)}, u32[]{:S(2)}) collective-permute-start(bf16[352,768]{1,0:T(8,128)(2,1)S(1)} %shard_map.165.own), channel_id=1, source_target_pairs={{32,0},{64,32},{96,64},{128,96},{160,128},{192,160},{224,192},{256... | collective-permute-start | bytes 1622024 | tf_op jit(solution)/shard_map/ppermute | solution.py:25
  44.0 15.1 %collective-permute-start.5 = (bf16[352,768]{1,0:T(8,128)(2,1)S(1)}, bf16[352,768]{1,0:T(8,128)(2,1)S(1)}, u32[]{:S(2)}, u32[]{:S(2)}) collective-permute-start(bf16[352,768]{1,0:T(8,128)(2,1)S(1)} %collective-permute-done.3.m1), channel_id=1, source_target_pairs={{992,0},{0,32},{32,64},{64,96},{96,128},{128,160},{160,192},{192,2... | collective-permute-start | bytes 1622024 | tf_op jit(solution)/shard_map/ppermute | solution.py:25
  51.0 26.2 %collective-permute-start.11 = (bf16[480,768]{1,0:T(8,128)(2,1)S(1)}, bf16[480,768]{1,0:T(8,128)(2,1)S(1)}, u32[]{:S(2)}, u32[]{:S(2)}) collective-permute-start(bf16[480,768]{1,0:T(8,128)(2,1)S(1)} %shard_map.168.rest_0_), channel_id=1, source_target_pairs={{24,0},{0,8},{8,16},{16,24},{25,1},{1,9},{9,17},{17,25},{26,2},{2,... | collective-permute-start | bytes 2211848 | tf_op jit(solution)/shard_map/ppermute | solution.py:25
  53.8 12.6 %collective-permute-start.4 = (bf16[352,768]{1,0:T(8,128)(2,1)S(1)}, bf16[352,768]{1,0:T(8,128)(2,1)S(1)}, u32[]{:S(2)}, u32[]{:S(2)}) collective-permute-start(bf16[352,768]{1,0:T(8,128)(2,1)S(1)} %collective-permute-done.1.p1), channel_id=1, source_target_pairs={{32,0},{64,32},{96,64},{128,96},{160,128},{192,160},{224,192},{256... | collective-permute-start | bytes 1622024 | tf_op jit(solution)/shard_map/ppermute | solution.py:25
  59.2 12.7 %collective-permute-start.7 = (bf16[304,768]{1,0:T(8,128)(2,1)S(1)}, bf16[304,768]{1,0:T(8,128)(2,1)S(1)}, u32[]{:S(2)}, u32[]{:S(2)}) collective-permute-start(bf16[304,768]{1,0:T(8,128)(2,1)S(1)} %slice.13), channel_id=1, source_target_pairs={{992,0},{0,32},{32,64},{64,96},{96,128},{128,160},{160,192},{192,2... | collective-permute-start | bytes 1400840 | tf_op jit(solution)/shard_map/ppermute | solution.py:25
  61.1 20.1 %collective-permute-start.10 = (bf16[480,768]{1,0:T(8,128)(2,1)S(1)}, bf16[480,768]{1,0:T(8,128)(2,1)S(1)}, u32[]{:S(2)}, u32[]{:S(2)}) collective-permute-start(bf16[480,768]{1,0:T(8,128)(2,1)S(1)} %shard_map.168.rest_0_), channel_id=1, source_target_pairs={{8,0},{16,8},{24,16},{0,24},{9,1},{17,9},{25,17},{1,25},{10,2},{18... | collective-permute-start | bytes 2211848 | tf_op jit(solution)/shard_map/ppermute | solution.py:25
  66.4 14.3 %copy-start = (bf16[256,2048]{1,0:T(8,128)(2,1)S(1)}, bf16[256,2048]{1,0:T(8,128)(2,1)}, u32[]{:S(2)}) copy-start(bf16[256,2048]{1,0:T(8,128)(2,1)} %stream.5) | copy-start | bytes 3145732
  66.4 18.6 %collective-permute-start.6 = (bf16[304,768]{1,0:T(8,128)(2,1)S(1)}, bf16[304,768]{1,0:T(8,128)(2,1)S(1)}, u32[]{:S(2)}, u32[]{:S(2)}) collective-permute-start(bf16[304,768]{1,0:T(8,128)(2,1)S(1)} %slice.12), channel_id=1, source_target_pairs={{32,0},{64,32},{96,64},{128,96},{160,128},{192,160},{224,192},{256... | collective-permute-start | bytes 1400840 | tf_op jit(solution)/shard_map/ppermute | solution.py:25
  71.9 8.7 %copy-start.8 = (f32[352]{0:T(512)S(1)}, f32[352]{0:T(512)}, u32[]{:S(2)}) copy-start(f32[352]{0:T(512)} %param.27) | copy-start | bytes 4228
  71.9 8.8 %copy-start.1 = (f32[128,128]{1,0:T(8,128)S(1)}, f32[128,128]{1,0:T(8,128)}, u32[]{:S(2)}) copy-start(f32[128,128]{1,0:T(8,128)} %constant.5.clone.sine) | copy-start | bytes 196612
  71.9 8.8 %copy-start.2 = (f32[128,128]{1,0:T(8,128)S(1)}, f32[128,128]{1,0:T(8,128)}, u32[]{:S(2)}) copy-start(f32[128,128]{1,0:T(8,128)} %constant.4.clone.cosine) | copy-start | bytes 196612
  72.0 19.7 %collective-permute-start.8 = (bf16[256,768]{1,0:T(8,128)(2,1)S(1)}, bf16[256,768]{1,0:T(8,128)(2,1)S(1)}, u32[]{:S(2)}, u32[]{:S(2)}) collective-permute-start(bf16[256,768]{1,0:T(8,128)(2,1)S(1)} %slice.14), channel_id=1, source_target_pairs={{992,0},{0,32},{32,64},{64,96},{96,128},{128,160},{160,192},{192,2... | collective-permute-start | bytes 1179656 | tf_op jit(solution)/shard_map/ppermute | solution.py:25
  74.0 6.6 %copy-start.9 = (f32[352]{0:T(512)S(1)}, f32[352]{0:T(512)}, u32[]{:S(2)}) copy-start(f32[352]{0:T(512)} %param.29) | copy-start | bytes 4228
  74.0 6.7 %copy-start.5 = (f32[256]{0:T(256)S(1)}, f32[256]{0:T(256)}, u32[]{:S(2)}) copy-start(f32[256]{0:T(256)} %param.20) | copy-start | bytes 3076
  74.0 6.7 %copy-start.6 = (f32[256]{0:T(256)S(1)}, f32[256]{0:T(256)}, u32[]{:S(2)}) copy-start(f32[256]{0:T(256)} %param.22) | copy-start | bytes 3076
  74.1 6.7 %copy-start.7 = (f32[256]{0:T(256)S(1)}, f32[256]{0:T(256)}, u32[]{:S(2)}) copy-start(f32[256]{0:T(256)} %param.24) | copy-start | bytes 3076
  74.1 6.6 %copy-start.3 = (f32[2048]{0:T(1024)S(1)}, f32[2048]{0:T(1024)}, u32[]{:S(2)}) copy-start(f32[2048]{0:T(1024)} %param.18) | copy-start | bytes 24580
  74.1 6.6 %copy-start.4 = (f32[2048]{0:T(1024)S(1)}, f32[2048]{0:T(1024)}, u32[]{:S(2)}) copy-start(f32[2048]{0:T(1024)} %param.25) | copy-start | bytes 24580
  74.1 8.7 %collective-permute-start.13 = (bf16[192,768]{1,0:T(8,128)(2,1)S(1)}, bf16[192,768]{1,0:T(8,128)(2,1)S(1)}, u32[]{:S(2)}, u32[]{:S(2)}) collective-permute-start(bf16[192,768]{1,0:T(8,128)(2,1)S(1)} %shard_map.169.rest_3_), channel_id=1, source_target_pairs={{24,0},{0,8},{8,16},{16,24},{25,1},{1,9},{9,17},{17,25},{26,2},{2,... | collective-permute-start | bytes 884744 | tf_op jit(solution)/shard_map/ppermute | solution.py:25
  77.2 7.8 %collective-permute-start.12 = (bf16[192,768]{1,0:T(8,128)(2,1)S(1)}, bf16[192,768]{1,0:T(8,128)(2,1)S(1)}, u32[]{:S(2)}, u32[]{:S(2)}) collective-permute-start(bf16[192,768]{1,0:T(8,128)(2,1)S(1)} %shard_map.169.rest_3_), channel_id=1, source_target_pairs={{8,0},{16,8},{24,16},{0,24},{9,1},{17,9},{25,17},{1,25},{10,2},{18... | collective-permute-start | bytes 884744 | tf_op jit(solution)/shard_map/ppermute | solution.py:25
  85.1 39.9 %collective-permute-start.15 = (bf16[432,768]{1,0:T(8,128)(2,1)S(1)}, bf16[432,768]{1,0:T(8,128)(2,1)S(1)}, u32[]{:S(2)}, u32[]{:S(2)}) collective-permute-start(bf16[432,768]{1,0:T(8,128)(2,1)S(1)} %get-tuple-element.28), channel_id=1, source_target_pairs={{24,0},{0,8},{8,16},{16,24},{25,1},{1,9},{9,17},{17,25},{26,2},{2,... | collective-permute-start | bytes 1990664 | tf_op jit(solution)/shard_map/ppermute | solution.py:25
  87.9 37.1 %collective-permute-start.14 = (bf16[432,768]{1,0:T(8,128)(2,1)S(1)}, bf16[432,768]{1,0:T(8,128)(2,1)S(1)}, u32[]{:S(2)}, u32[]{:S(2)}) collective-permute-start(bf16[432,768]{1,0:T(8,128)(2,1)S(1)} %get-tuple-element.27.rest_6_), channel_id=1, source_target_pairs={{8,0},{16,8},{24,16},{0,24},{9,1},{17,9},{25,17},{1,25},{10,2},{18... | collective-permute-start | bytes 1990664 | tf_op jit(solution)/shard_map/ppermute | solution.py:25
  105.1 20.8 %collective-permute-start.9 = (bf16[4,256,256]{2,1,0:T(8,128)(2,1)S(1)}, bf16[4,256,256]{2,1,0:T(8,128)(2,1)S(1)}, u32[]{:S(2)}, u32[]{:S(2)}) collective-permute-start(bf16[4,256,256]{2,1,0:T(8,128)(2,1)S(1)} %bitcast.10), channel_id=1, source_target_pairs={{1,0},{0,1},{3,2},{2,3},{5,4},{4,5},{7,6},{6,7},{9,8},{8,9},{11,10... | collective-permute-start | bytes 1572872 | tf_op jit(solution)/shard_map/ppermute | solution.py:25
  116.2 8.8 %collective-permute-start.16 = (bf16[96,768]{1,0:T(8,128)(2,1)S(1)}, bf16[96,768]{1,0:T(8,128)(2,1)S(1)}, u32[]{:S(2)}, u32[]{:S(2)}) collective-permute-start(bf16[96,768]{1,0:T(8,128)(2,1)S(1)} %get-tuple-element.29), channel_id=1, source_target_pairs={{16,0},{24,8},{0,16},{8,24},{17,1},{25,9},{1,17},{9,25},{18,2},{26... | collective-permute-start | bytes 442376 | tf_op jit(solution)/shard_map/ppermute | solution.py:25
  127.7 4.3 %collective-permute-start.17 = (bf16[128,2048]{1,0:T(8,128)(2,1)S(1)}, bf16[128,2048]{1,0:T(8,128)(2,1)S(1)}, u32[]{:S(2)}, u32[]{:S(2)}) collective-permute-start(bf16[128,2048]{1,0:T(8,128)(2,1)S(1)} %get-tuple-element.35), channel_id=1, source_target_pairs={{1,0},{0,1},{3,2},{2,3},{5,4},{4,5},{7,6},{6,7},{9,8},{8,9},{11,10... | collective-permute-start | bytes 1572872 | tf_op jit(solution)/shard_map/ppermute | solution.py:25

commit v3 on v2

--- a/solution.py
+++ b/solution.py
@@ -156,7 +156,8 @@
         retained = jnp.dot(scores * mask, value[rows], precision=HIGH, preferred_element_type=F32)
         square = jnp.mean(retained * retained, axis=-1, keepdims=True)
         mixed = (retained * (1.0 / jnp.maximum(jnp.sqrt(square), 1.0))).astype(BF16)
-        out[rows, :] = mixed
+        for copy in range(4):
+            out[copy, rows, :] = mixed
 
 
 NAMES = ("a0", "ap", "am", "b0", "bp", "bm", "c0", "cp", "cm", "d2")
@@ -326,17 +327,17 @@
     p3, m3 = shift(p2[0:304], Z, 1), shift(m2[0:304], Z, -1)
     b0 = call(round_b_kernel, rows_of(192), p2, m2)
     bp, bm = shift(b0, "y", 1), shift(b0, "y", -1)
-    p4 = shift(m3[0:256], Z, -1)
+    p4 = shift(p3[0:256], Z, 1)
     c0, c0_m, last = call(round_c_kernel, (rows_of(432), rows_of(432), rows_of(96)), p3, m3, bp, bm, ap, am)
     cp, cm = shift(c0, "y", 1), shift(c0_m, "y", -1)
     d2 = shift(last, "y", 2)
 
     mixed = call(
         retention_kernel,
-        jax.ShapeDtypeStruct((256, 256), BF16),
+        jax.ShapeDtypeStruct((4, 256, 256), BF16),
         normed, own, p1, m1, p2, m2, p3, m3, p4, scales, tables,
     )
-    heads = lax.all_gather(mixed, "x", axis=0)
+    heads = lax.all_to_all(mixed, "x", split_axis=0, concat_axis=0, tiled=True)
     others = shift(heads, "c", 1)
     shards_of_ffn = (a0, ap, am, b0, bp, bm, c0, cp, cm, d2)
     own_resid, own_acc, own_total = call(

time: 146 us -> 157 us (1.075)
  starting transfers between devices: 72.9 us -> 91.5 us
  waiting for transfers between devices: 39.1 us -> 26.8 us
  blocking collectives: 23 us -> 13.6 us
  Pallas kernels: 9.19 us -> 17 us
  local copies, waits for them, and re-layouts: 0.16 us -> 6.17 us
    ppermute x18, starting transfers between devices: 67.9 us -> 82.3 us  [shift(): return lax.ppermute(array, axis, [((i + offset) % n, i) for i in range(n)])]
    ppermute x18, waiting for transfers between devices: 39 us -> 26.8 us  [shift(): return lax.ppermute(array, axis, [((i + offset) % n, i) for i in range(n)])]
    all_gather x1 -> x0, blocking collectives: 11.1 us -> none  [shards(): heads = lax.all_gather(mixed, 'x', axis=0)]
    pallas_call x13, Pallas kernels: 9.19 us -> 17 us  [call(): pl.pallas_call(kernel, out_shape=out_shape, in_specs=specs or [VMEM] * le...]
    unnamed x20 -> x42, local copies, waits for them, and re-layouts: 0.06 us -> 6.07 us
    all_to_all x0 -> x1, starting transfers between devices: none -> 4.14 us  [shards(): heads = lax.all_to_all(mixed, 'x', split_axis=0, concat_axis=0, tiled=True)]
    all_to_all x1, blocking collectives: 11.8 us -> 13.6 us  [shards(): lax.all_to_all(partial, 'x', split_axis=0, concat_axis=0, tiled=True)]
  transfers between devices with their start and end apart: 19 -> 20, of which waited for: 9 -> 8; matrix products, arithmetic and copies ran while one was open for 0% -> 0% of each run, Pallas kernels for 3% -> 7%
where the time goes in v3:
time: 157 us; the launch traced here: 156 us
  starting transfers between devices  91.5 us (58%)
  waiting for transfers between devices  26.8 us (17%)
  Pallas kernels  17 us (11%)
  blocking collectives  13.6 us (9%)
  local copies, waits for them, and re-layouts  6.17 us (4%)
    ppermute x18, starting transfers between devices, shift(): return lax.ppermute(array, axis, [((i + offset) % n, i) for i in range(n)])  82.3 us
    ppermute x18, waiting for transfers between devices, shift(): return lax.ppermute(array, axis, [((i + offset) % n, i) for i in range(n)])  26.8 us
    pallas_call x13, Pallas kernels, call(): pl.pallas_call(kernel, out_shape=out_shape, in_specs=specs or [VMEM] * le...  17 us
    all_to_all x1, blocking collectives, shards(): lax.all_to_all(partial, 'x', split_axis=0, concat_axis=0, tiled=True)  13.6 us
    unnamed x42, local copies, waits for them, and re-layouts  6.07 us
    all_to_all x1, starting transfers between devices, shards(): lax.all_to_all(qkv, 'y', split_axis=0, concat_axis=0, tiled=True)  5.01 us
    all_to_all x1, starting transfers between devices, shards(): heads = lax.all_to_all(mixed, 'x', split_axis=0, concat_axis=0, tiled=True)  4.14 us
  transfers between devices with their start and end apart: 20, of which 8 were waited for; matrix products, arithmetic and copies ran while one was open for 0% of the time, Pallas kernels for 7%

profile of v3, /device:TPU:1, one launch (start us, length us, event | category | flops | bytes accessed | tf_op | source)
XLA Modules:
  0.0 155.5 jit_solution(10553569548775541283)
XLA Ops:
  0.0 1.9 %shard_map.164 = (bf16[4,64,768]{2,1,0:T(8,128)(2,1)}, bf16[96,768]{1,0:T(8,128)(2,1)S(1)}) custom-call(f32[64,256]{1,0:T(8,128)} %refs_0_.1, f32[64,256]{1,0:T(8,128)} %refs_1_.1, f32[64,256]{1,0:T(8,128)} %refs_2_.1, f32[64,352]{1,0:T(8,128)} %refs_3_.1, f32[64,352]{1,0:T(8,128)} %refs_4_.1, f32[64,352]{1,0:T(8,128)} %refs_5_.1, f32[1,64]{1,0:T(1,128)} %bitcast.14), custom_call_target="tpu_custom_call" | custom-call | tf_op jit(solution)/shard_map/pallas_call | solution.py:29
  1.9 5.0 %all-to-all-start = ((bf16[4,64,768]{2,1,0:T(8,128)(2,1)}), bf16[4,64,768]{2,1,0:T(8,128)(2,1)S(1)}, u32[]{:S(2)}, u32[]{:S(2)}) async-start(bf16[4,64,768]{2,1,0:T(8,128)(2,1)} %get-tuple-element.22), calls=%async_computation | async-start | bytes 786432 | tf_op jit(solution)/shard_map/all_to_all | solution.py:307
  6.9 18.4 %collective-permute-start = (bf16[96,768]{1,0:T(8,128)(2,1)S(1)}, bf16[96,768]{1,0:T(8,128)(2,1)S(1)}, u32[]{:S(2)}, u32[]{:S(2)}) collective-permute-start(bf16[96,768]{1,0:T(8,128)(2,1)S(1)} %get-tuple-element.23.own), channel_id=1, source_target_pairs={{32,0},{64,32},{96,64},{128,96},{160,128},{192,160},{224,192},{256... | collective-permute-start | bytes 442376 | tf_op jit(solution)/shard_map/ppermute | solution.py:25
  25.3 2.1 %collective-permute-done.ffn.fp1 = bf16[96,768]{1,0:T(8,128)(2,1)S(1)} collective-permute-done((bf16[96,768]{1,0:T(8,128)(2,1)S(1)}, bf16[96,768]{1,0:T(8,128)(2,1)S(1)}, u32[]{:S(2)}, u32[]{:S(2)}) %collective-permute-start) | collective-permute-done | bytes 147488 | tf_op jit(solution)/shard_map/ppermute | solution.py:25
  27.4 0.0 all-to-all-done
  27.5 5.5 %collective-permute-start.1 = (bf16[352,768]{1,0:T(8,128)(2,1)S(1)}, bf16[352,768]{1,0:T(8,128)(2,1)S(1)}, u32[]{:S(2)}, u32[]{:S(2)}) collective-permute-start(bf16[352,768]{1,0:T(8,128)(2,1)S(1)} %shard_map.165.own), channel_id=1, source_target_pairs={{32,0},{64,32},{96,64},{128,96},{160,128},{192,160},{224,192},{256... | collective-permute-start | bytes 1622024 | tf_op jit(solution)/shard_map/ppermute | solution.py:25
  32.9 1.9 %collective-permute-start.2 = (bf16[96,768]{1,0:T(8,128)(2,1)S(1)}, bf16[96,768]{1,0:T(8,128)(2,1)S(1)}, u32[]{:S(2)}, u32[]{:S(2)}) collective-permute-start(bf16[96,768]{1,0:T(8,128)(2,1)S(1)} %get-tuple-element.23.own), channel_id=1, source_target_pairs={{992,0},{0,32},{32,64},{64,96},{96,128},{128,160},{160,192},{192,2... | collective-permute-start | bytes 442376 | tf_op jit(solution)/shard_map/ppermute | solution.py:25
  34.9 5.2 %collective-permute-done.2.ffn.fm1 = bf16[96,768]{1,0:T(8,128)(2,1)S(1)} collective-permute-done((bf16[96,768]{1,0:T(8,128)(2,1)S(1)}, bf16[96,768]{1,0:T(8,128)(2,1)S(1)}, u32[]{:S(2)}, u32[]{:S(2)}) %collective-permute-start.2) | collective-permute-done | bytes 147488 | tf_op jit(solution)/shard_map/ppermute | solution.py:25
  40.1 1.9 %collective-permute-start.3 = (bf16[352,768]{1,0:T(8,128)(2,1)S(1)}, bf16[352,768]{1,0:T(8,128)(2,1)S(1)}, u32[]{:S(2)}, u32[]{:S(2)}) collective-permute-start(bf16[352,768]{1,0:T(8,128)(2,1)S(1)} %shard_map.166), channel_id=1, source_target_pairs={{992,0},{0,32},{32,64},{64,96},{96,128},{128,160},{160,192},{192,2... | collective-permute-start | bytes 1622024 | tf_op jit(solution)/shard_map/ppermute | solution.py:25
  42.0 0.7 collective-permute-done.1.p1
  42.7 5.3 %collective-permute-start.4 = (bf16[352,768]{1,0:T(8,128)(2,1)S(1)}, bf16[352,768]{1,0:T(8,128)(2,1)S(1)}, u32[]{:S(2)}, u32[]{:S(2)}) collective-permute-start(bf16[352,768]{1,0:T(8,128)(2,1)S(1)} %collective-permute-done.1.p1), channel_id=1, source_target_pairs={{32,0},{64,32},{96,64},{128,96},{160,128},{192,160},{224,192},{256... | collective-permute-start | bytes 1622024 | tf_op jit(solution)/shard_map/ppermute | solution.py:25
  48.1 5.7 %collective-permute-done.3.m1 = bf16[352,768]{1,0:T(8,128)(2,1)S(1)} collective-permute-done((bf16[352,768]{1,0:T(8,128)(2,1)S(1)}, bf16[352,768]{1,0:T(8,128)(2,1)S(1)}, u32[]{:S(2)}, u32[]{:S(2)}) %collective-permute-start.3) | collective-permute-done | bytes 540704 | tf_op jit(solution)/shard_map/ppermute | solution.py:25
  53.8 1.9 %collective-permute-start.5 = (bf16[352,768]{1,0:T(8,128)(2,1)S(1)}, bf16[352,768]{1,0:T(8,128)(2,1)S(1)}, u32[]{:S(2)}, u32[]{:S(2)}) collective-permute-start(bf16[352,768]{1,0:T(8,128)(2,1)S(1)} %collective-permute-done.3.m1), channel_id=1, source_target_pairs={{992,0},{0,32},{32,64},{64,96},{96,128},{128,160},{160,192},{192,2... | collective-permute-start | bytes 1622024 | tf_op jit(solution)/shard_map/ppermute | solution.py:25
  55.7 1.3 collective-permute-done.4.p2
  57.0 5.3 %collective-permute-start.6 = (bf16[304,768]{1,0:T(8,128)(2,1)S(1)}, bf16[304,768]{1,0:T(8,128)(2,1)S(1)}, u32[]{:S(2)}, u32[]{:S(2)}) collective-permute-start(bf16[304,768]{1,0:T(8,128)(2,1)S(1)} %slice.12), channel_id=1, source_target_pairs={{32,0},{64,32},{96,64},{128,96},{160,128},{192,160},{224,192},{256... | collective-permute-start | bytes 1400840 | tf_op jit(solution)/shard_map/ppermute | solution.py:25
  62.4 4.2 %collective-permute-done.5.m2 = bf16[352,768]{1,0:T(8,128)(2,1)S(1)} collective-permute-done((bf16[352,768]{1,0:T(8,128)(2,1)S(1)}, bf16[352,768]{1,0:T(8,128)(2,1)S(1)}, u32[]{:S(2)}, u32[]{:S(2)}) %collective-permute-start.5) | collective-permute-done | bytes 540704 | tf_op jit(solution)/shard_map/ppermute | solution.py:25
  66.6 1.9 %collective-permute-start.7 = (bf16[304,768]{1,0:T(8,128)(2,1)S(1)}, bf16[304,768]{1,0:T(8,128)(2,1)S(1)}, u32[]{:S(2)}, u32[]{:S(2)}) collective-permute-start(bf16[304,768]{1,0:T(8,128)(2,1)S(1)} %slice.13), channel_id=1, source_target_pairs={{992,0},{0,32},{32,64},{64,96},{96,128},{128,160},{160,192},{192,2... | collective-permute-start | bytes 1400840 | tf_op jit(solution)/shard_map/ppermute | solution.py:25
  68.6 0.1 shard_map.168.rest_0_
  68.6 0.0 copy-start
  68.6 3.1 %collective-permute-start.10 = (bf16[480,768]{1,0:T(8,128)(2,1)S(1)}, bf16[480,768]{1,0:T(8,128)(2,1)S(1)}, u32[]{:S(2)}, u32[]{:S(2)}) collective-permute-start(bf16[480,768]{1,0:T(8,128)(2,1)S(1)} %shard_map.168.rest_0_), channel_id=1, source_target_pairs={{8,0},{16,8},{24,16},{0,24},{9,1},{17,9},{25,17},{1,25},{10,2},{18... | collective-permute-start | bytes 2211848 | tf_op jit(solution)/shard_map/ppermute | solution.py:25
  71.7 2.3 %collective-permute-start.11 = (bf16[480,768]{1,0:T(8,128)(2,1)S(1)}, bf16[480,768]{1,0:T(8,128)(2,1)S(1)}, u32[]{:S(2)}, u32[]{:S(2)}) collective-permute-start(bf16[480,768]{1,0:T(8,128)(2,1)S(1)} %shard_map.168.rest_0_), channel_id=1, source_target_pairs={{24,0},{0,8},{8,16},{16,24},{25,1},{1,9},{9,17},{17,25},{26,2},{2,... | collective-permute-start | bytes 2211848 | tf_op jit(solution)/shard_map/ppermute | solution.py:25
  74.1 0.0 collective-permute-done.6.p3
  74.1 0.0 copy-start.19
  74.1 0.0 copy-start.6
  74.1 0.0 copy-start.7
  74.2 4.7 %collective-permute-start.8 = (bf16[256,768]{1,0:T(8,128)(2,1)S(1)}, bf16[256,768]{1,0:T(8,128)(2,1)S(1)}, u32[]{:S(2)}, u32[]{:S(2)}) collective-permute-start(bf16[256,768]{1,0:T(8,128)(2,1)S(1)} %slice.14), channel_id=1, source_target_pairs={{32,0},{64,32},{96,64},{128,96},{160,128},{192,160},{224,192},{256... | collective-permute-start | bytes 1179656 | tf_op jit(solution)/shard_map/ppermute | solution.py:25
  78.9 0.0 copy-start.20
  78.9 0.0 copy-start.15
  78.9 0.0 copy-start.16
  78.9 0.0 copy-start.17
  78.9 0.8 shard_map.169.rest_3_
  79.7 4.3 %collective-permute-start.12 = (bf16[192,768]{1,0:T(8,128)(2,1)}, bf16[192,768]{1,0:T(8,128)(2,1)S(1)}, u32[]{:S(2)}, u32[]{:S(2)}) collective-permute-start(bf16[192,768]{1,0:T(8,128)(2,1)} %shard_map.169.rest_3_), channel_id=1, source_target_pairs={{8,0},{16,8},{24,16},{0,24},{9,1},{17,9},{25,17},{1,25},{10,2},{18... | collective-permute-start | bytes 884744 | tf_op jit(solution)/shard_map/ppermute | solution.py:25
  84.0 0.0 collective-permute-done.7.m3
  84.0 1.9 %collective-permute-start.13 = (bf16[192,768]{1,0:T(8,128)(2,1)}, bf16[192,768]{1,0:T(8,128)(2,1)}, u32[]{:S(2)}, u32[]{:S(2)}) collective-permute-start(bf16[192,768]{1,0:T(8,128)(2,1)} %shard_map.169.rest_3_), channel_id=1, source_target_pairs={{24,0},{0,8},{8,16},{16,24},{25,1},{1,9},{9,17},{17,25},{26,2},{2,... | collective-permute-start | bytes 884744 | tf_op jit(solution)/shard_map/ppermute | solution.py:25
  86.1 0.4 shard_map.163
  86.5 0.0 copy-start.8
  86.5 0.6 copy-done.8
  87.1 0.6 copy-done.13
  87.7 2.3 %shard_map.167 = bf16[4,256,256]{2,1,0:T(8,128)(2,1)S(1)} custom-call(bf16[256,2048]{1,0:T(8,128)(2,1)S(1)} %get-tuple-element.21.normed, bf16[352,768]{1,0:T(8,128)(2,1)S(1)} %shard_map.165.own, bf16[352,768]{1,0:T(8,128)(2,1)S(1)} %collective-permute-done.1.p1, bf16[352,768]{1,0:T(8,128)(2,1)S(1)} %collective-permute-done.3.m1, ...), custom_call_target="tpu_custom_call" | custom-call | tf_op jit(solution)/shard_map/pallas_call | solution.py:29
  90.0 0.8 copy-done.3
  90.8 4.1 %all-to-all-start.1 = ((bf16[4,256,256]{2,1,0:T(8,128)(2,1)}), bf16[4,256,256]{2,1,0:T(8,128)(2,1)}, u32[]{:S(2)}, u32[]{:S(2)}) async-start(bf16[4,256,256]{2,1,0:T(8,128)(2,1)} %copy-done.3), calls=%async_computation.1 | async-start | bytes 1048576 | tf_op jit(solution)/shard_map/all_to_all | solution.py:340
  94.9 0.0 collective-permute-done.10.ap.rest_1_
  94.9 0.0 collective-permute-done.11.am.rest_2_
  95.0 1.4 collective-permute-done.13.bm.rest_5_
  96.4 1.0 copy-done.2
  97.4 1.0 copy-done.5
  98.4 2.1 %shard_map.170 = (bf16[432,768]{1,0:T(8,128)(2,1)}, bf16[432,768]{1,0:T(8,128)(2,1)}, bf16[96,768]{1,0:T(8,128)(2,1)S(1)}) custom-call(bf16[304,768]{1,0:T(8,128)(2,1)S(1)} %copy-done.2, bf16[304,768]{1,0:T(8,128)(2,1)S(1)} %copy-done.5, bf16[192,768]{1,0:T(8,128)(2,1)S(1)} %collective-permute-done.12.bp.rest_4_, ...), custom_call_target="tpu_custom_call" | custom-call | tf_op jit(solution)/shard_map/pallas_call | solution.py:29
  100.5 0.7 copy-done.18
  101.2 3.2 %collective-permute-start.14 = (bf16[432,768]{1,0:T(8,128)(2,1)}, bf16[432,768]{1,0:T(8,128)(2,1)}, u32[]{:S(2)}, u32[]{:S(2)}) collective-permute-start(bf16[432,768]{1,0:T(8,128)(2,1)} %get-tuple-element.27.rest_6_), channel_id=1, source_target_pairs={{8,0},{16,8},{24,16},{0,24},{9,1},{17,9},{25,17},{1,25},{10,2},{18... | collective-permute-start | bytes 1990664 | tf_op jit(solution)/shard_map/ppermute | solution.py:25
  104.3 2.1 %collective-permute-start.15 = (bf16[432,768]{1,0:T(8,128)(2,1)}, bf16[432,768]{1,0:T(8,128)(2,1)}, u32[]{:S(2)}, u32[]{:S(2)}) collective-permute-start(bf16[432,768]{1,0:T(8,128)(2,1)} %get-tuple-element.28), channel_id=1, source_target_pairs={{24,0},{0,8},{8,16},{16,24},{25,1},{1,9},{9,17},{17,25},{26,2},{2,... | collective-permute-start | bytes 1990664 | tf_op jit(solution)/shard_map/ppermute | solution.py:25
  106.4 9.4 %collective-permute-start.9 = (bf16[4,256,256]{2,1,0:T(8,128)(2,1)}, bf16[4,256,256]{2,1,0:T(8,128)(2,1)S(1)}, u32[]{:S(2)}, u32[]{:S(2)}) collective-permute-start(bf16[4,256,256]{2,1,0:T(8,128)(2,1)} %all-to-all-done.1.heads), channel_id=1, source_target_pairs={{1,0},{0,1},{3,2},{2,3},{5,4},{4,5},{7,6},{6,7},{9,8},{8,9},{11,10... | collective-permute-start | bytes 1572872 | tf_op jit(solution)/shard_map/ppermute | solution.py:25
  115.8 3.1 %collective-permute-start.16 = (bf16[96,768]{1,0:T(8,128)(2,1)}, bf16[96,768]{1,0:T(8,128)(2,1)S(1)}, u32[]{:S(2)}, u32[]{:S(2)}) collective-permute-start(bf16[96,768]{1,0:T(8,128)(2,1)} %copy-done.18), channel_id=1, source_target_pairs={{16,0},{24,8},{0,16},{8,24},{17,1},{25,9},{1,17},{9,25},{18,2},{26... | collective-permute-start | bytes 442376 | tf_op jit(solution)/shard_map/ppermute | solution.py:25
  118.9 6.1 %collective-permute-done.16.rest_9_ = bf16[96,768]{1,0:T(8,128)(2,1)S(1)} collective-permute-done((bf16[96,768]{1,0:T(8,128)(2,1)}, bf16[96,768]{1,0:T(8,128)(2,1)S(1)}, u32[]{:S(2)}, u32[]{:S(2)}) %collective-permute-start.16) | collective-permute-done | bytes 147488 | tf_op jit(solution)/shard_map/ppermute | solution.py:25
  125.0 0.0 collective-permute-done.14.rest_7_
  125.0 0.0 collective-permute-done.15.rest_8_
  125.0 0.7 copy-done.9
  125.7 2.7 %shard_map.171 = (f32[4,256,256]{2,1,0:T(8,128)S(1)}, f32[256,768]{1,0:T(8,128)S(1)}, f32[256,1]{1,0:T(8,128)S(1)}) custom-call(bf16[256,2048]{1,0:T(8,128)(2,1)S(1)} %copy-done, bf16[4,256,256]{2,1,0:T(8,128)(2,1)} %all-to-all-done.1.heads, f32[8,1,256]{2,1,0:T(1,128)S(1)} %copy-done.9, bf16[480,768]{1,0:T(8,128)(2,1)S(1)} %shard_map.168.rest_0_, ...), custom_call_target="tpu_custom_call" | custom-call | tf_op jit(solution)/shard_map/pallas_call | solution.py:29
  128.5 0.6 copy-done.14
  129.1 3.4 %shard_map.172 = (bf16[128,2048]{1,0:T(8,128)(2,1)S(1)}, bf16[128,384]{1,0:T(8,128)(2,1)S(1)}, f32[32,2048]{1,0:T(8,128)S(1)}) custom-call(bf16[256,2048]{1,0:T(8,128)(2,1)S(1)} %copy-done, bf16[4,256,256]{2,1,0:T(8,128)(2,1)S(1)} %collective-permute-done.9.heads, f32[8,1,256]{2,1,0:T(1,128)S(1)} %copy-done.10, ...), custom_call_target="tpu_custom_call" | custom-call | tf_op jit(solution)/shard_map/pallas_call | solution.py:29
  132.5 6.1 %collective-permute-start.17 = (bf16[128,2048]{1,0:T(8,128)(2,1)S(1)}, bf16[128,2048]{1,0:T(8,128)(2,1)S(1)}, u32[]{:S(2)}, u32[]{:S(2)}) collective-permute-start(bf16[128,2048]{1,0:T(8,128)(2,1)S(1)} %get-tuple-element.35), channel_id=1, source_target_pairs={{1,0},{0,1},{3,2},{2,3},{5,4},{4,5},{7,6},{6,7},{9,8},{8,9},{11,10... | collective-permute-start | bytes 1572872 | tf_op jit(solution)/shard_map/ppermute | solution.py:25
  138.7 2.4 %shard_map.173.keep = f32[128,2048]{1,0:T(8,128)S(1)} custom-call(bf16[128,384]{1,0:T(8,128)(2,1)S(1)} %get-tuple-element.34.hidden, bf16[480,768]{1,0:T(8,128)(2,1)S(1)} %shard_map.168.rest_0_, bf16[480,768]{1,0:T(8,128)(2,1)S(1)} %collective-permute-done.10.ap.rest_1_, bf16[480,768]{1,0:T(8,128)(2,1)S(1)} %collective-permute-done.11.am.rest_2_, ...), custom_call_target="tpu_custom_call" | custom-call | tf_op jit(solution)/shard_map/pallas_call | solution.py:29
  141.0 0.1 shard_map.174
  141.1 13.6 %all_to_all.15.arrived = bf16[4,32,2048]{2,1,0:T(8,128)(2,1)S(1)} all-to-all(bf16[4,32,2048]{2,1,0:T(8,128)(2,1)S(1)} %shard_map.174), channel_id=1, replica_groups=mesh['zh'=4,'zl'=8,'y'=4,'x'=4,'c'=2] {'x'}, dimensions={0} | all-to-all | bytes 1048576 | tf_op jit(solution)/shard_map/all_to_all | solution.py:362
  154.7 0.8 shard_map.175
  (37 shorter events, 0.2 us)
Async XLA Ops:
  1.9 25.5 %all-to-all-start = ((bf16[4,64,768]{2,1,0:T(8,128)(2,1)}), bf16[4,64,768]{2,1,0:T(8,128)(2,1)S(1)}, u32[]{:S(2)}, u32[]{:S(2)}) async-start(bf16[4,64,768]{2,1,0:T(8,128)(2,1)} %get-tuple-element.22), calls=%async_computation | async-start | bytes 786432 | tf_op jit(solution)/shard_map/all_to_all | solution.py:307
  6.9 20.5 %collective-permute-start = (bf16[96,768]{1,0:T(8,128)(2,1)S(1)}, bf16[96,768]{1,0:T(8,128)(2,1)S(1)}, u32[]{:S(2)}, u32[]{:S(2)}) collective-permute-start(bf16[96,768]{1,0:T(8,128)(2,1)S(1)} %get-tuple-element.23.own), channel_id=1, source_target_pairs={{32,0},{64,32},{96,64},{128,96},{160,128},{192,160},{224,192},{256... | collective-permute-start | bytes 442376 | tf_op jit(solution)/shard_map/ppermute | solution.py:25
  27.5 15.3 %collective-permute-start.1 = (bf16[352,768]{1,0:T(8,128)(2,1)S(1)}, bf16[352,768]{1,0:T(8,128)(2,1)S(1)}, u32[]{:S(2)}, u32[]{:S(2)}) collective-permute-start(bf16[352,768]{1,0:T(8,128)(2,1)S(1)} %shard_map.165.own), channel_id=1, source_target_pairs={{32,0},{64,32},{96,64},{128,96},{160,128},{192,160},{224,192},{256... | collective-permute-start | bytes 1622024 | tf_op jit(solution)/shard_map/ppermute | solution.py:25
  32.9 7.1 %collective-permute-start.2 = (bf16[96,768]{1,0:T(8,128)(2,1)S(1)}, bf16[96,768]{1,0:T(8,128)(2,1)S(1)}, u32[]{:S(2)}, u32[]{:S(2)}) collective-permute-start(bf16[96,768]{1,0:T(8,128)(2,1)S(1)} %get-tuple-element.23.own), channel_id=1, source_target_pairs={{992,0},{0,32},{32,64},{64,96},{96,128},{128,160},{160,192},{192,2... | collective-permute-start | bytes 442376 | tf_op jit(solution)/shard_map/ppermute | solution.py:25
  40.1 13.7 %collective-permute-start.3 = (bf16[352,768]{1,0:T(8,128)(2,1)S(1)}, bf16[352,768]{1,0:T(8,128)(2,1)S(1)}, u32[]{:S(2)}, u32[]{:S(2)}) collective-permute-start(bf16[352,768]{1,0:T(8,128)(2,1)S(1)} %shard_map.166), channel_id=1, source_target_pairs={{992,0},{0,32},{32,64},{64,96},{96,128},{128,160},{160,192},{192,2... | collective-permute-start | bytes 1622024 | tf_op jit(solution)/shard_map/ppermute | solution.py:25
  42.7 14.3 %collective-permute-start.4 = (bf16[352,768]{1,0:T(8,128)(2,1)S(1)}, bf16[352,768]{1,0:T(8,128)(2,1)S(1)}, u32[]{:S(2)}, u32[]{:S(2)}) collective-permute-start(bf16[352,768]{1,0:T(8,128)(2,1)S(1)} %collective-permute-done.1.p1), channel_id=1, source_target_pairs={{32,0},{64,32},{96,64},{128,96},{160,128},{192,160},{224,192},{256... | collective-permute-start | bytes 1622024 | tf_op jit(solution)/shard_map/ppermute | solution.py:25
  53.8 12.8 %collective-permute-start.5 = (bf16[352,768]{1,0:T(8,128)(2,1)S(1)}, bf16[352,768]{1,0:T(8,128)(2,1)S(1)}, u32[]{:S(2)}, u32[]{:S(2)}) collective-permute-start(bf16[352,768]{1,0:T(8,128)(2,1)S(1)} %collective-permute-done.3.m1), channel_id=1, source_target_pairs={{992,0},{0,32},{32,64},{64,96},{96,128},{128,160},{160,192},{192,2... | collective-permute-start | bytes 1622024 | tf_op jit(solution)/shard_map/ppermute | solution.py:25
  57.0 17.0 %collective-permute-start.6 = (bf16[304,768]{1,0:T(8,128)(2,1)S(1)}, bf16[304,768]{1,0:T(8,128)(2,1)S(1)}, u32[]{:S(2)}, u32[]{:S(2)}) collective-permute-start(bf16[304,768]{1,0:T(8,128)(2,1)S(1)} %slice.12), channel_id=1, source_target_pairs={{32,0},{64,32},{96,64},{128,96},{160,128},{192,160},{224,192},{256... | collective-permute-start | bytes 1400840 | tf_op jit(solution)/shard_map/ppermute | solution.py:25
  66.6 17.4 %collective-permute-start.7 = (bf16[304,768]{1,0:T(8,128)(2,1)S(1)}, bf16[304,768]{1,0:T(8,128)(2,1)S(1)}, u32[]{:S(2)}, u32[]{:S(2)}) collective-permute-start(bf16[304,768]{1,0:T(8,128)(2,1)S(1)} %slice.13), channel_id=1, source_target_pairs={{992,0},{0,32},{32,64},{64,96},{96,128},{128,160},{160,192},{192,2... | collective-permute-start | bytes 1400840 | tf_op jit(solution)/shard_map/ppermute | solution.py:25
  68.6 17.4 %copy-start = (bf16[256,2048]{1,0:T(8,128)(2,1)S(1)}, bf16[256,2048]{1,0:T(8,128)(2,1)}, u32[]{:S(2)}) copy-start(bf16[256,2048]{1,0:T(8,128)(2,1)} %stream.5) | copy-start | bytes 3145732
  68.6 26.3 %collective-permute-start.10 = (bf16[480,768]{1,0:T(8,128)(2,1)S(1)}, bf16[480,768]{1,0:T(8,128)(2,1)S(1)}, u32[]{:S(2)}, u32[]{:S(2)}) collective-permute-start(bf16[480,768]{1,0:T(8,128)(2,1)S(1)} %shard_map.168.rest_0_), channel_id=1, source_target_pairs={{8,0},{16,8},{24,16},{0,24},{9,1},{17,9},{25,17},{1,25},{10,2},{18... | collective-permute-start | bytes 2211848 | tf_op jit(solution)/shard_map/ppermute | solution.py:25
  71.7 23.2 %collective-permute-start.11 = (bf16[480,768]{1,0:T(8,128)(2,1)S(1)}, bf16[480,768]{1,0:T(8,128)(2,1)S(1)}, u32[]{:S(2)}, u32[]{:S(2)}) collective-permute-start(bf16[480,768]{1,0:T(8,128)(2,1)S(1)} %shard_map.168.rest_0_), channel_id=1, source_target_pairs={{24,0},{0,8},{8,16},{16,24},{25,1},{1,9},{9,17},{17,25},{26,2},{2,... | collective-permute-start | bytes 2211848 | tf_op jit(solution)/shard_map/ppermute | solution.py:25
  74.1 13.6 %copy-start.1 = (bf16[304,768]{1,0:T(8,128)(2,1)}, bf16[304,768]{1,0:T(8,128)(2,1)S(1)}, u32[]{:S(2)}) copy-start(bf16[304,768]{1,0:T(8,128)(2,1)S(1)} %collective-permute-done.6.p3) | copy-start | bytes 1400836
  74.1 11.8 %copy-start.19 = (f32[352]{0:T(512)S(1)}, f32[352]{0:T(512)}, u32[]{:S(2)}) copy-start(f32[352]{0:T(512)} %param.27) | copy-start | bytes 4228
  74.1 11.9 %copy-start.6 = (f32[128,128]{1,0:T(8,128)S(1)}, f32[128,128]{1,0:T(8,128)}, u32[]{:S(2)}) copy-start(f32[128,128]{1,0:T(8,128)} %constant.4.clone.cosine) | copy-start | bytes 196612
  74.1 11.9 %copy-start.7 = (f32[128,128]{1,0:T(8,128)S(1)}, f32[128,128]{1,0:T(8,128)}, u32[]{:S(2)}) copy-start(f32[128,128]{1,0:T(8,128)} %constant.5.clone.sine) | copy-start | bytes 196612
  74.2 12.9 %collective-permute-start.8 = (bf16[256,768]{1,0:T(8,128)(2,1)S(1)}, bf16[256,768]{1,0:T(8,128)(2,1)S(1)}, u32[]{:S(2)}, u32[]{:S(2)}) collective-permute-start(bf16[256,768]{1,0:T(8,128)(2,1)S(1)} %slice.14), channel_id=1, source_target_pairs={{32,0},{64,32},{96,64},{128,96},{160,128},{192,160},{224,192},{256... | collective-permute-start | bytes 1179656 | tf_op jit(solution)/shard_map/ppermute | solution.py:25
  78.9 7.1 %copy-start.20 = (f32[352]{0:T(512)S(1)}, f32[352]{0:T(512)}, u32[]{:S(2)}) copy-start(f32[352]{0:T(512)} %param.29) | copy-start | bytes 4228
  78.9 7.1 %copy-start.15 = (f32[256]{0:T(256)S(1)}, f32[256]{0:T(256)}, u32[]{:S(2)}) copy-start(f32[256]{0:T(256)} %param.20) | copy-start | bytes 3076
  78.9 7.1 %copy-start.16 = (f32[256]{0:T(256)S(1)}, f32[256]{0:T(256)}, u32[]{:S(2)}) copy-start(f32[256]{0:T(256)} %param.22) | copy-start | bytes 3076
  78.9 7.1 %copy-start.17 = (f32[256]{0:T(256)S(1)}, f32[256]{0:T(256)}, u32[]{:S(2)}) copy-start(f32[256]{0:T(256)} %param.24) | copy-start | bytes 3076
  79.7 6.4 %copy-start.11 = (f32[2048]{0:T(1024)S(1)}, f32[2048]{0:T(1024)}, u32[]{:S(2)}) copy-start(f32[2048]{0:T(1024)} %param.18) | copy-start | bytes 24580
  79.7 6.4 %copy-start.12 = (f32[2048]{0:T(1024)S(1)}, f32[2048]{0:T(1024)}, u32[]{:S(2)}) copy-start(f32[2048]{0:T(1024)} %param.25) | copy-start | bytes 24580
  79.7 15.3 %collective-permute-start.12 = (bf16[192,768]{1,0:T(8,128)(2,1)}, bf16[192,768]{1,0:T(8,128)(2,1)S(1)}, u32[]{:S(2)}, u32[]{:S(2)}) collective-permute-start(bf16[192,768]{1,0:T(8,128)(2,1)} %shard_map.169.rest_3_), channel_id=1, source_target_pairs={{8,0},{16,8},{24,16},{0,24},{9,1},{17,9},{25,17},{1,25},{10,2},{18... | collective-permute-start | bytes 884744 | tf_op jit(solution)/shard_map/ppermute | solution.py:25
  84.0 3.7 %copy-start.4 = (bf16[304,768]{1,0:T(8,128)(2,1)}, bf16[304,768]{1,0:T(8,128)(2,1)S(1)}, u32[]{:S(2)}) copy-start(bf16[304,768]{1,0:T(8,128)(2,1)S(1)} %collective-permute-done.7.m3) | copy-start | bytes 1400836
  84.0 12.3 %collective-permute-start.13 = (bf16[192,768]{1,0:T(8,128)(2,1)}, bf16[192,768]{1,0:T(8,128)(2,1)}, u32[]{:S(2)}, u32[]{:S(2)}) collective-permute-start(bf16[192,768]{1,0:T(8,128)(2,1)} %shard_map.169.rest_3_), channel_id=1, source_target_pairs={{24,0},{0,8},{8,16},{16,24},{25,1},{1,9},{9,17},{17,25},{26,2},{2,... | collective-permute-start | bytes 884744 | tf_op jit(solution)/shard_map/ppermute | solution.py:25
  86.5 0.6 copy-start.8
  87.1 0.6 copy-start.13
  90.0 0.8 copy-start.3
  90.8 15.7 %all-to-all-start.1 = ((bf16[4,256,256]{2,1,0:T(8,128)(2,1)}), bf16[4,256,256]{2,1,0:T(8,128)(2,1)}, u32[]{:S(2)}, u32[]{:S(2)}) async-start(bf16[4,256,256]{2,1,0:T(8,128)(2,1)} %copy-done.3), calls=%async_computation.1 | async-start | bytes 1048576 | tf_op jit(solution)/shard_map/all_to_all | solution.py:340
  96.4 1.0 copy-start.2
  97.4 1.0 copy-start.5
  100.5 0.7 copy-start.18
  101.2 23.8 %collective-permute-start.14 = (bf16[432,768]{1,0:T(8,128)(2,1)}, bf16[432,768]{1,0:T(8,128)(2,1)}, u32[]{:S(2)}, u32[]{:S(2)}) collective-permute-start(bf16[432,768]{1,0:T(8,128)(2,1)} %get-tuple-element.27.rest_6_), channel_id=1, source_target_pairs={{8,0},{16,8},{24,16},{0,24},{9,1},{17,9},{25,17},{1,25},{10,2},{18... | collective-permute-start | bytes 1990664 | tf_op jit(solution)/shard_map/ppermute | solution.py:25
  104.3 20.7 %collective-permute-start.15 = (bf16[432,768]{1,0:T(8,128)(2,1)}, bf16[432,768]{1,0:T(8,128)(2,1)}, u32[]{:S(2)}, u32[]{:S(2)}) collective-permute-start(bf16[432,768]{1,0:T(8,128)(2,1)} %get-tuple-element.28), channel_id=1, source_target_pairs={{24,0},{0,8},{8,16},{16,24},{25,1},{1,9},{9,17},{17,25},{26,2},{2,... | collective-permute-start | bytes 1990664 | tf_op jit(solution)/shard_map/ppermute | solution.py:25
  106.4 22.0 %collective-permute-start.9 = (bf16[4,256,256]{2,1,0:T(8,128)(2,1)}, bf16[4,256,256]{2,1,0:T(8,128)(2,1)S(1)}, u32[]{:S(2)}, u32[]{:S(2)}) collective-permute-start(bf16[4,256,256]{2,1,0:T(8,128)(2,1)} %all-to-all-done.1.heads), channel_id=1, source_target_pairs={{1,0},{0,1},{3,2},{2,3},{5,4},{4,5},{7,6},{6,7},{9,8},{8,9},{11,10... | collective-permute-start | bytes 1572872 | tf_op jit(solution)/shard_map/ppermute | solution.py:25
  115.8 9.2 %collective-permute-start.16 = (bf16[96,768]{1,0:T(8,128)(2,1)}, bf16[96,768]{1,0:T(8,128)(2,1)S(1)}, u32[]{:S(2)}, u32[]{:S(2)}) collective-permute-start(bf16[96,768]{1,0:T(8,128)(2,1)} %copy-done.18), channel_id=1, source_target_pairs={{16,0},{24,8},{0,16},{8,24},{17,1},{25,9},{1,17},{9,25},{18,2},{26... | collective-permute-start | bytes 442376 | tf_op jit(solution)/shard_map/ppermute | solution.py:25
  125.0 0.7 copy-start.9
  125.7 2.8 %copy-start.10 = (f32[8,1,256]{2,1,0:T(1,128)S(1)}, f32[8,1,256]{2,1,0:T(1,128)}, u32[]{:S(2)}) copy-start(f32[8,1,256]{2,1,0:T(1,128)} %copy-done.8) | copy-start | bytes 24580
  128.4 0.7 copy-start.14
  132.5 8.5 %collective-permute-start.17 = (bf16[128,2048]{1,0:T(8,128)(2,1)S(1)}, bf16[128,2048]{1,0:T(8,128)(2,1)S(1)}, u32[]{:S(2)}, u32[]{:S(2)}) collective-permute-start(bf16[128,2048]{1,0:T(8,128)(2,1)S(1)} %get-tuple-element.35), channel_id=1, source_target_pairs={{1,0},{0,1},{3,2},{2,3},{5,4},{4,5},{7,6},{6,7},{9,8},{8,9},{11,10... | collective-permute-start | bytes 1572872 | tf_op jit(solution)/shard_map/ppermute | solution.py:25
